TPU v7x, 256 devices: a 4x2x16 block of a 4x16x16 slice. The times are simulated.
256 devices in a mesh: grp: 2 (over y), sp: 32 (over z, core), tp: 4 (over x).
Axes of the slice: x: 4, y: 2, z: 16, core: 2. Of those that a mesh axis runs over, the one named last changes fastest.
The devices are a block of a 4x16x16 slice.
Arguments:
- stream: bfloat16 [32768, 2048], P(('grp', 'sp')), parts along dimension 0, may hold values from -6 to 6
- queries_a: bfloat16 [32768, 512], P(('grp', 'sp'), 'tp'), parts along dimension 0, may hold values from -6 to 6
- keys_a: bfloat16 [32768, 512], P(('grp', 'sp'), 'tp'), parts along dimension 0, may hold values from -6 to 6
- queries_b: bfloat16 [32768, 1024], P(('grp', 'sp'), 'tp'), parts along dimension 0, may hold values from -6 to 6
- keys_b: bfloat16 [32768, 1024], P(('grp', 'sp'), 'tp'), parts along dimension 0, may hold values from -6 to 6
- values: bfloat16 [32768, 2, 1024], P(('grp', 'sp'), None, 'tp'), parts along dimension 0, may hold values from -6 to 6
- out_gate: bfloat16 [32768, 2, 1024], P(('grp', 'sp'), None, 'tp'), parts along dimension 0, may hold values from -6 to 6
- in_gate: float32 [2, 8, 32768], P(None, 'tp', ('grp', 'sp')), parts along dimension 2, may hold values from -4 to 250
- forget_gate: float32 [2, 8, 32768], P(None, 'tp', ('grp', 'sp')), parts along dimension 2, may hold values from -5 to 16
- head_gain: float32 [2, 1024], P(None, 'tp'), may hold values from 0.1 to 1.9
- out_weight: bfloat16 [2, 1024, 2048], P(None, 'tp'), may hold values from -0.125 to 0.125
- norm_gain: float32 [2048], replicated, may hold values from 0.1 to 1.9
- gate_weight: bfloat16 [2048, 5632], P('sp', 'tp'), may hold values from -0.125 to 0.125
- up_weight: bfloat16 [2048, 5632], P('sp', 'tp'), may hold values from -0.125 to 0.125
- down_weight: bfloat16 [5632, 2048], P('tp', 'sp'), may hold values from -0.078125 to 0.078125
Outputs:
- layer_out: bfloat16 [32768, 2048], P(('grp', 'sp', 'tp')), parts along dimension 0
There are 2 independent parts, one for each index of `grp`. A program takes and returns all parts, laid end to end along the dimension named above; an argument that names none is the same for every part. Nothing has to cross between parts.
All inputs are finite; a program needn't handle non-finite values.
Results may differ from a plain program's by a relative error of at most 0.013.
Values may be sent and summed in bfloat16 or wider, within the bound.
A program may use at most 128 MiB of HBM per device.

v0:
```python
import jax
import jax.numpy as jnp
from jax import lax
from jax.sharding import Mesh
from jax.sharding import PartitionSpec as P

SP = ("sp_0", "sp_1")
GRP_SP = ("grp", "sp_0", "sp_1")
GRP_SP_TP = ("grp", "sp_0", "sp_1", "tp")


EPS = 1e-06
NEG = -1e30
HIGHEST = lax.Precision.HIGHEST


def rows_first(arrays, axis, dims):
    turned = [jnp.moveaxis(a, dim, 0) for a, dim in zip(arrays, dims)]
    both = jnp.concatenate([t.reshape(len(t), -1) for t in turned], axis=1)
    result, at, gathered = (lax.all_gather(both, axis, axis=0, tiled=True), 0, [])
    for t, dim in zip(turned, dims):
        piece = result[:, at : at + t[0].size].reshape(-1, *t.shape[1:])
        gathered.append(jnp.moveaxis(piece, 0, dim))
        at += t[0].size
    return tuple(gathered)


def filled_with(value, identity):
    return jax.tree.map(
        lambda part, zero: jnp.zeros_like(part) + jnp.asarray(zero, part.dtype), value, identity
    )


def collected_together(value, axis):
    leaves = jax.tree.leaves(value)
    order = sorted(range(len(leaves)), key=lambda k: -leaves[k].size)
    width = (1, *leaves[order[0]].shape)[-1]
    lines = [
        jnp.pad(leaves[k].reshape(-1), (0, -leaves[k].size % width)).reshape(-1, width)
        for k in order
    ]
    both, at, found = (lax.all_gather(jnp.concatenate(lines), axis), 0, {})
    for k, line in zip(order, lines):
        piece = both[:, at : at + len(line)].reshape(len(both), -1)
        found[k] = piece[:, : leaves[k].size].reshape(-1, *leaves[k].shape)
        at += len(line)
    numbers = iter(range(len(leaves)))
    return jax.tree.map(lambda _: found[next(numbers)], value)


def prefix_by_axis(value, axes, combine, identity):
    before = start = filled_with(value, identity)
    so_far = value
    for axis in reversed(axes):
        size, here = (lax.axis_size(axis), lax.axis_index(axis))
        pieces = collected_together(so_far, axis)
        inside, so_far = (start, start)
        for k in range(size):
            passed = k < here
            so_far = combine(so_far, jax.tree.map(lambda part: part[k], pieces))
            inside = jax.tree.map(lambda new, old: jnp.where(passed, new, old), so_far, inside)
        before = combine(inside, before)
    return before


def from_everyone(value, axis):
    size = lax.axis_size(axis)
    return lax.all_to_all(
        jnp.broadcast_to(value[None], (size, *value.shape)), axis, 0, 0, tiled=True
    )


def of_everyone(value, axis):
    everything = from_everyone(value, axis)
    return jnp.sum(everything, axis=0)


def in_blocks(value, dim, size):
    before, after = (value.shape[:dim], value.shape[dim + 1 :])
    return jnp.moveaxis(value.reshape(*before, size, -1, *after), dim, 0)


def sum_at_owner(value, axis, dim):
    size = lax.axis_size(axis)
    blocks = lax.all_to_all(in_blocks(value, dim, size), axis, 0, 0, tiled=True)
    return jnp.sum(blocks.astype(jnp.float32), axis=0)


def in_order(blocks, dim):
    blocks = jnp.moveaxis(blocks, 0, dim)
    lengths = blocks.shape
    return blocks.reshape(*lengths[:dim], lengths[dim] * lengths[dim + 1], *lengths[dim + 2 :])


def gather_directly(value, axis, dim):
    return in_order(from_everyone(value, axis), dim)


def block_state(key_rows, values, in_rates, forget_rates):
    cumul = jnp.cumsum(jax.nn.log_sigmoid(forget_rates), axis=1)
    total = cumul[:, -1]
    tail = total[:, None] - cumul + in_rates
    peak = jnp.max(tail, axis=1)
    weight = jnp.exp(tail - peak[:, None])
    weighted = (values.astype(jnp.float32) * jnp.transpose(weight)[:, :, None]).astype(jnp.bfloat16)
    state = jnp.einsum("rhv,rhk->hvk", weighted, key_rows, preferred_element_type=jnp.float32)
    norm_vec = jnp.einsum("hr,rhk->hk", weight, key_rows.astype(jnp.float32), precision=HIGHEST)
    return ((state, norm_vec, peak, total), cumul)


def read_block(queries, key_rows, values, in_rates, cumul, carried, scale):
    length = queries.shape[0]
    scores = (
        jnp.einsum("rhk,shk->hrs", queries, key_rows, preferred_element_type=jnp.float32) * scale
    )
    causal = lax.broadcasted_iota(jnp.int32, (length, length), 0) >= lax.broadcasted_iota(
        jnp.int32, (length, length), 1
    )
    decay_log = cumul[:, :, None] - cumul[:, None, :] + in_rates[:, None, :]
    decay_log = jnp.where(causal[None], decay_log, -jnp.inf)
    carried_log = cumul + carried[2][:, None]
    stabil = jnp.maximum(carried_log, jnp.max(decay_log, axis=2))
    weight_matrices = scores * jnp.exp(decay_log - stabil[:, :, None])
    carried_weight = jnp.exp(carried_log - stabil) * scale
    query_wide = queries.astype(jnp.float32)
    denom = jnp.sum(weight_matrices, axis=2) + carried_weight * jnp.einsum(
        "hk,rhk->hr", carried[1], query_wide, precision=HIGHEST
    )
    numer = jnp.einsum(
        "hrs,shv->rhv",
        weight_matrices.astype(jnp.bfloat16),
        values,
        preferred_element_type=jnp.float32,
    )
    numer = numer + jnp.transpose(carried_weight)[:, :, None] * jnp.einsum(
        "hvk,rhk->rhv", carried[0], query_wide, precision=HIGHEST
    )
    floor_val = jnp.maximum(jnp.abs(denom), jnp.exp(-stabil))
    return numer / jnp.transpose(floor_val)[:, :, None]


def combine_group(earlier, later):
    peak = jnp.maximum(later[3] + earlier[2], later[2])
    initial_scale = jnp.exp(later[3] + earlier[2] - peak)
    late_scale = jnp.exp(later[2] - peak)
    state = initial_scale[:, None, None] * earlier[0] + late_scale[:, None, None] * later[0]
    norm_vec = initial_scale[:, None] * earlier[1] + late_scale[:, None] * later[1]
    return (state, norm_vec, peak, earlier[3] + later[3])


def combine_both(earlier, later):
    return combine_group(earlier[:4], later[:4]) + combine_group(earlier[4:], later[4:])


def head_output(cell, mean_square, gain, gate):
    lines = cell.shape[0]
    normed = cell * lax.rsqrt(mean_square + EPS)[:, None, None]
    return (normed.reshape(lines, -1) * gain * jax.nn.sigmoid(gate.astype(jnp.float32))).astype(
        jnp.bfloat16
    )


def rms_normed(residual, gain):
    return (
        residual * lax.rsqrt(jnp.mean(residual * residual, axis=1, keepdims=True) + EPS) * gain
    ).astype(jnp.bfloat16)


def local(
    stream,
    queries_a,
    keys_a,
    queries_b,
    keys_b,
    values,
    out_gate,
    in_gate,
    forget_gate,
    head_gain,
    out_weight,
    norm_gain,
    gate_weight,
    up_weight,
    down_weight,
):
    gate_whole, up_whole, down_whole = rows_first(
        (gate_weight, up_weight, down_weight), SP, (0, 0, 1)
    )
    length = stream.shape[0]
    heads = in_gate.shape[1]
    value_size = values.shape[2] // heads
    prepared = []
    own_states = []
    for group, (queries, key_rows) in enumerate(((queries_a, keys_a), (queries_b, keys_b))):
        key_size = queries.shape[1] // heads
        query_heads = queries.reshape(length, heads, key_size)
        key_heads = key_rows.reshape(length, heads, key_size)
        value_heads = values[:, group].reshape(length, heads, value_size)
        own, cumul = block_state(key_heads, value_heads, in_gate[group], forget_gate[group])
        own_states.append(own)
        prepared.append((query_heads, key_heads, value_heads, cumul, key_size))
    first_own, second_own = own_states
    size_first = prepared[0][4]
    size_second = prepared[1][4]
    carried = prefix_by_axis(
        (
            first_own[0],
            first_own[1],
            first_own[2],
            first_own[3],
            second_own[0],
            second_own[1],
            second_own[2],
            second_own[3],
        ),
        SP,
        combine_both,
        (
            jnp.zeros((heads, value_size, size_first), jnp.float32),
            jnp.zeros((heads, size_first), jnp.float32),
            jnp.full((heads,), NEG, jnp.float32),
            jnp.zeros((heads,), jnp.float32),
            jnp.zeros((heads, value_size, size_second), jnp.float32),
            jnp.zeros((heads, size_second), jnp.float32),
            jnp.full((heads,), NEG, jnp.float32),
            jnp.zeros((heads,), jnp.float32),
        ),
    )
    cells = []
    for group in range(2):
        query_heads, key_heads, value_heads, cumul, key_size = prepared[group]
        cells.append(
            read_block(
                query_heads,
                key_heads,
                value_heads,
                in_gate[group],
                cumul,
                carried[4 * group : 4 * group + 3],
                key_size ** (-0.5),
            )
        )
    cell_first, cell_second = cells
    square_first = jnp.sum(cell_first * cell_first, axis=(1, 2))
    square_second = jnp.sum(cell_second * cell_second, axis=(1, 2))
    total_first, total_second = (of_everyone(square_first, "tp"), of_everyone(square_second, "tp"))
    group_columns = heads * lax.axis_size("tp") * value_size
    mixed_first = head_output(cell_first, total_first / group_columns, head_gain[0], out_gate[:, 0])
    mixed_second = head_output(
        cell_second, total_second / group_columns, head_gain[1], out_gate[:, 1]
    )
    share = length // lax.axis_size("tp")
    own_start = lax.axis_index("tp") * share
    mixture = sum_at_owner(
        (
            jnp.dot(mixed_first, out_weight[0], preferred_element_type=jnp.float32)
            + jnp.dot(mixed_second, out_weight[1], preferred_element_type=jnp.float32)
        ).astype(jnp.bfloat16),
        "tp",
        0,
    )
    residual_own = (
        lax.dynamic_slice_in_dim(stream, own_start, share, 0).astype(jnp.float32) + mixture
    )
    ffn_inputs = gather_directly(rms_normed(residual_own, norm_gain), "tp", 0)
    gate = jnp.dot(ffn_inputs, gate_whole, preferred_element_type=jnp.float32)
    up_proj = jnp.dot(ffn_inputs, up_whole, preferred_element_type=jnp.float32)
    active = (jax.nn.silu(gate) * up_proj).astype(jnp.bfloat16)
    ffn_term = jnp.dot(active, down_whole, preferred_element_type=jnp.float32)
    ffn_rows_sum = sum_at_owner(ffn_term.astype(jnp.bfloat16), "tp", 0)
    return (residual_own + ffn_rows_sum).astype(jnp.bfloat16)


def solution(mesh):
    finer = Mesh(
        mesh.devices.reshape(mesh.shape["grp"], 16, 2, mesh.shape["tp"]),
        ("grp", "sp_0", "sp_1", "tp"),
    )
    return jax.shard_map(
        local,
        mesh=finer,
        in_specs=(
            P(GRP_SP, None),
            P(GRP_SP, "tp"),
            P(GRP_SP, "tp"),
            P(GRP_SP, "tp"),
            P(GRP_SP, "tp"),
            P(GRP_SP, None, "tp"),
            P(GRP_SP, None, "tp"),
            P(None, "tp", GRP_SP),
            P(None, "tp", GRP_SP),
            P(None, "tp"),
            P(None, "tp", None),
            P(),
            P(SP, "tp"),
            P(SP, "tp"),
            P("tp", SP),
        ),
        out_specs=P(GRP_SP_TP, None),
        check_vma=False,
    )
```

profile of v0, /device:TPU:33, one launch (start us, length us, event | category | flops | bytes accessed | tf_op | source)
XLA Modules:
  0.0 273.8 jit_solution(18407314016636816470)
XLA Ops:
  10.8 2.2 fusion.492
  15.8 22.3 %all-gather.2 = f32[2,391,128]{2,1,0:T(8,128)S(1)} all-gather(f32[1,391,128]{2,1,0:T(8,128)S(1)} %bitcast.1019), channel_id=2, replica_groups=mesh['grp'=2,'sp_0'=16,'sp_1'=2,'tp'=4] {'sp_1'}, dimensions={0}, use_global_device_ids=true | all-gather | bytes 600576 | tf_op jit(solution)/shard_map/all_gather | solution.py:42
  40.5 1.9 concatenate.10
  48.4 1.3 add_divide_fusion
  49.6 1.4 fusion.15
  51.0 51.0 %all-gather.9.cloned.1.call-done = f32[16,391,128]{2,1,0:T(8,128)} async-done(((f32[1,391,128]{2,1,0:T(8,128)}), f32[16,391,128]{2,1,0:T(8,128)}) %all-gather.9.cloned.1.call-update) | async-done | bytes 3203088 | tf_op jit(solution)/shard_map/all_gather | solution.py:42
  102.1 1.7 fusion.489
  104.0 1.0 fusion.339
  105.2 2.1 fusion.498
  109.4 1.1 multiply_reduce_fusion.1
  111.1 4.1 %all-to-all-start.1 = ((f32[4,1,512]{2,1,0:T(1,128)}), f32[4,1,512]{2,1,0:T(1,128)}, u32[]{:S(2)}, u32[]{:S(2)}) async-start(f32[4,1,512]{2,1,0:T(1,128)} %broadcast_in_dim.35), calls=%async_computation.1 | async-start | bytes 16384 | tf_op jit(solution)/shard_map/all_to_all | solution.py:68
  115.2 1.0 fusion.490
  124.3 0.9 squeeze.510
  139.1 0.9 squeeze.519
  142.1 1.1 subtract_exponential_fusion.69
  143.8 1.0 subtract_exponential_fusion.53
  147.8 2.3 fusion.497
  151.1 1.1 multiply_reduce_fusion.2
  152.9 4.2 %all-to-all-start = ((f32[4,1,512]{2,1,0:T(1,128)}), f32[4,1,512]{2,1,0:T(1,128)S(1)}, u32[]{:S(2)}, u32[]{:S(2)}) async-start(f32[4,1,512]{2,1,0:T(1,128)} %broadcast_in_dim.32), calls=%async_computation | async-start | bytes 16384 | tf_op jit(solution)/shard_map/all_to_all | solution.py:68
  158.3 2.9 %all-to-all-done = f32[4,1,512]{2,1,0:T(1,128)S(1)} async-done(((f32[4,1,512]{2,1,0:T(1,128)}), f32[4,1,512]{2,1,0:T(1,128)S(1)}, u32[]{:S(2)}, u32[]{:S(2)}) %all-to-all-start) | async-done | bytes 8224 | tf_op jit(solution)/shard_map/all_to_all | solution.py:68
  161.3 1.2 multiply_convert_fusion.1
  162.5 1.2 multiply_convert_fusion.2
  164.4 2.1 add_convert_fusion
  166.5 3.7 %all-to-all-start.2 = ((bf16[4,128,2048]{2,1,0:T(8,128)(2,1)}), bf16[4,128,2048]{2,1,0:T(8,128)(2,1)S(1)}, u32[]{:S(2)}, u32[]{:S(2)}) async-start(bf16[4,128,2048]{2,1,0:T(8,128)(2,1)} %bitcast.1002), calls=%async_computation.2 | async-start | bytes 4194304 | tf_op jit(solution)/shard_map/all_to_all | solution.py:85
  170.3 15.3 %all-to-all-done.2 = bf16[4,128,2048]{2,1,0:T(8,128)(2,1)S(1)} async-done(((bf16[4,128,2048]{2,1,0:T(8,128)(2,1)}), bf16[4,128,2048]{2,1,0:T(8,128)(2,1)S(1)}, u32[]{:S(2)}, u32[]{:S(2)}) %all-to-all-start.2) | async-done | bytes 2097184 | tf_op jit(solution)/shard_map/all_to_all | solution.py:85
  186.0 1.2 copy-done.10
  187.9 20.9 %all_to_all.27 = bf16[4,128,2048]{2,1,0:T(8,128)(2,1)S(1)} all-to-all(bf16[4,128,2048]{2,1,0:T(8,128)(2,1)S(1)} %broadcast_in_dim.36), channel_id=1, replica_groups=mesh['grp'=2,'sp_0'=16,'sp_1'=2,'tp'=4] {'tp'}, dimensions={0} | all-to-all | bytes 4194304 | tf_op jit(solution)/shard_map/all_to_all | solution.py:68
  208.8 9.0 %all-gather.7.cloned.1.call-done = bf16[2048,4224]{1,0:T(8,128)(2,1)} async-done(((bf16[64,4224]{1,0:T(8,128)(2,1)}), bf16[2048,4224]{1,0:T(8,128)(2,1)}) %all-gather.7.cloned.1.call-update) | async-done | bytes 17301520 | tf_op jit(solution)/shard_map/all_gather | solution.py:20
  217.8 7.6 %fusion.4 = f32[512,1408]{1,0:T(8,128)} fusion(bf16[512,2048]{1,0:T(8,128)(2,1)S(1)} %bitcast.1006, bf16[2048,4224]{1,0:T(8,128)(2,1)} %all-gather.7.cloned.1.call-done), kind=kOutput, calls=%fused_computation.4 | convolution fusion | flops 2952790016 | bytes 10747904 | tf_op jit(solution)/shard_map/dot_general | solution.py:266
  225.4 13.3 %fusion.12 = bf16[512,2048]{1,0:T(8,128)(2,1)} fusion(bf16[2048,4224]{1,0:T(8,128)(2,1)} %all-gather.7.cloned.1.call-done, bf16[512,2048]{1,0:T(8,128)(2,1)S(1)} %bitcast.1007, f32[512,1408]{1,0:T(8,128)} %fusion.4), kind=kOutput, calls=%fused_computation.11 | convolution fusion | flops 5910953984 | bytes 18612224 | tf_op jit(solution)/shard_map/dot_general | solution.py:269
  238.6 25.9 %all_to_all.28 = bf16[4,128,2048]{2,1,0:T(8,128)(2,1)S(1)} all-to-all(bf16[4,128,2048]{2,1,0:T(8,128)(2,1)} %bitcast.1008), channel_id=1, replica_groups=mesh['grp'=2,'sp_0'=16,'sp_1'=2,'tp'=4] {'tp'}, dimensions={0} | all-to-all | bytes 4194304 | tf_op jit(solution)/shard_map/all_to_all | solution.py:85
  264.9 2.0 add_convert_fusion.1
  (305 shorter events, 50.1 us)
Async XLA Ops:
  6.5 8.6 %copy-start = (bf16[512,256]{1,0:T(8,128)(2,1)S(1)}, bf16[512,256]{1,0:T(8,128)(2,1)}, u32[]{:S(2)}) copy-start(bf16[512,256]{1,0:T(8,128)(2,1)} %param.19) | copy-start | bytes 786436
  6.6 7.1 %copy-start.40 = (bf16[512,128]{1,0:T(8,128)(2,1)S(1)}, bf16[512,128]{1,0:T(8,128)(2,1)}, u32[]{:S(2)}) copy-start(bf16[512,128]{1,0:T(8,128)(2,1)} %param.17) | copy-start | bytes 393220
  6.6 95.5 %all-gather.9.cloned.1.call-start = ((), (), s32[]{:S(2)}) async-start(), calls=%async_computation.6 | async-start | bytes 3411968 | tf_op jit(solution)/shard_map/all_gather | solution.py:42
  8.4 41.2 %copy-start.42 = (f32[1,2,4,128]{3,1,2,0:T(2,128)}, f32[1,2,4,128]{3,1,2,0:T(2,128)S(1)}, u32[]{:S(2)}) copy-start(f32[1,2,4,128]{3,1,2,0:T(2,128)S(1)} %copy.249) | copy-start | bytes 12292
  9.7 39.9 %copy-start.44 = (f32[1,2,4,128]{3,1,2,0:T(2,128)}, f32[1,2,4,128]{3,1,2,0:T(2,128)S(1)}, u32[]{:S(2)}) copy-start(f32[1,2,4,128]{3,1,2,0:T(2,128)S(1)} %copy.248) | copy-start | bytes 12292
  13.7 25.8 %copy-start.11 = (bf16[512,1,256]{0,2,1:T(8,128)(2,1)}, bf16[512,1,256]{0,2,1:T(8,128)(2,1)S(1)}, u32[]{:S(2)}) copy-start(bf16[512,1,256]{0,2,1:T(8,128)(2,1)S(1)} %copy.139) | copy-start | bytes 786436
  14.9 25.5 %copy-start.17 = (bf16[512,1,256]{0,2,1:T(8,128)(2,1)}, bf16[512,1,256]{0,2,1:T(8,128)(2,1)S(1)}, u32[]{:S(2)}) copy-start(bf16[512,1,256]{0,2,1:T(8,128)(2,1)S(1)} %copy.137) | copy-start | bytes 786436
  15.7 26.8 %copy-start.37 = (bf16[1408,64]{0,1:T(8,128)(2,1)S(1)}, bf16[1408,64]{0,1:T(8,128)(2,1)}, u32[]{:S(2)}) copy-start(bf16[1408,64]{0,1:T(8,128)(2,1)} %param.29) | copy-start | bytes 540676
  15.7 26.8 %copy-start.38 = (bf16[64,1408]{1,0:T(8,128)(2,1)S(1)}, bf16[64,1408]{1,0:T(8,128)(2,1)}, u32[]{:S(2)}) copy-start(bf16[64,1408]{1,0:T(8,128)(2,1)} %param.28) | copy-start | bytes 540676
  15.7 26.8 %copy-start.39 = (bf16[64,1408]{1,0:T(8,128)(2,1)S(1)}, bf16[64,1408]{1,0:T(8,128)(2,1)}, u32[]{:S(2)}) copy-start(bf16[64,1408]{1,0:T(8,128)(2,1)} %param.27) | copy-start | bytes 540676
  38.1 5.3 %copy-start.50 = (f32[2]{0:T(128)}, f32[2]{0:T(128)S(1)}, u32[]{:S(2)}) copy-start(f32[2]{0:T(128)S(1)} %get-tuple-element.65) | copy-start | bytes 28
  38.6 4.8 %copy-start.52 = (f32[2]{0:T(128)}, f32[2]{0:T(128)S(1)}, u32[]{:S(2)}) copy-start(f32[2]{0:T(128)S(1)} %get-tuple-element.67) | copy-start | bytes 28
  38.6 4.8 %copy-start.54 = (f32[2]{0:T(128)}, f32[2]{0:T(128)S(1)}, u32[]{:S(2)}) copy-start(f32[2]{0:T(128)S(1)} %get-tuple-element.198) | copy-start | bytes 28
  38.7 4.8 %copy-start.60 = (f32[2]{0:T(128)}, f32[2]{0:T(128)S(1)}, u32[]{:S(2)}) copy-start(f32[2]{0:T(128)S(1)} %fusion.411) | copy-start | bytes 28
  39.5 4.1 %copy-start.36 = (bf16[512,256]{1,0:T(8,128)(2,1)S(1)}, bf16[512,256]{1,0:T(8,128)(2,1)}, u32[]{:S(2)}) copy-start(bf16[512,256]{1,0:T(8,128)(2,1)} %param.18) | copy-start | bytes 786436
  40.0 64.0 %copy-start.56 = (f32[2]{0:T(128)}, f32[2]{0:T(128)S(1)}, u32[]{:S(2)}) copy-start(f32[2]{0:T(128)S(1)} %get-tuple-element.204) | copy-start | bytes 28
  40.1 64.0 %copy-start.58 = (f32[2]{0:T(128)}, f32[2]{0:T(128)S(1)}, u32[]{:S(2)}) copy-start(f32[2]{0:T(128)S(1)} %get-tuple-element.209) | copy-start | bytes 28
  40.2 4.5 %copy-start.41 = (bf16[512,128]{1,0:T(8,128)(2,1)S(1)}, bf16[512,128]{1,0:T(8,128)(2,1)}, u32[]{:S(2)}) copy-start(bf16[512,128]{1,0:T(8,128)(2,1)} %param.16) | copy-start | bytes 393220
  40.5 6.4 %copy-start.45 = (f32[2,2,512]{2,1,0:T(2,128)S(1)}, f32[2,2,512]{2,1,0:T(2,128)}, u32[]{:S(2)}) copy-start(f32[2,2,512]{2,1,0:T(2,128)} %param.22) | copy-start | bytes 24580
  42.4 175.3 %all-gather.7.cloned.1.call-start = ((), (), s32[]{:S(2)}) async-start(), calls=%async_computation.5 | async-start | bytes 17842176 | tf_op jit(solution)/shard_map/all_gather | solution.py:20
  42.5 5.1 %copy-start.5 = (bf16[512,2,256]{2,1,0:T(2,128)(2,1)S(1)}, bf16[512,2,256]{2,1,0:T(2,128)(2,1)}, u32[]{:S(2)}) copy-start(bf16[512,2,256]{2,1,0:T(2,128)(2,1)} %param.21) | copy-start | bytes 1572868
  43.7 61.3 %copy-start.3 = (bf16[512,256]{0,1:T(8,128)(2,1)}, bf16[512,256]{0,1:T(8,128)(2,1)S(1)}, u32[]{:S(2)}) copy-start(bf16[512,256]{0,1:T(8,128)(2,1)S(1)} %copy.196) | copy-start | bytes 786436
  111.1 41.1 %all-to-all-start.1 = ((f32[4,1,512]{2,1,0:T(1,128)}), f32[4,1,512]{2,1,0:T(1,128)}, u32[]{:S(2)}, u32[]{:S(2)}) async-start(f32[4,1,512]{2,1,0:T(1,128)} %broadcast_in_dim.35), calls=%async_computation.1 | async-start | bytes 16384 | tf_op jit(solution)/shard_map/all_to_all | solution.py:68
  125.3 22.2 %copy-start.9 = (bf16[512,128]{0,1:T(8,128)(2,1)S(1)}, bf16[512,128]{0,1:T(8,128)(2,1)}, u32[]{:S(2)}) copy-start(bf16[512,128]{0,1:T(8,128)(2,1)} %copy.135) | copy-start | bytes 393220
  125.3 22.3 %copy-start.43 = (f32[1,2,4,128]{3,1,2,0:T(2,128)S(1)}, f32[1,2,4,128]{3,1,2,0:T(2,128)}, u32[]{:S(2)}) copy-start(f32[1,2,4,128]{3,1,2,0:T(2,128)} %copy-done.42) | copy-start | bytes 12292
  150.4 6.6 %copy-start.69 = (f32[2,256]{1,0:T(2,128)S(1)}, f32[2,256]{1,0:T(2,128)}, u32[]{:S(2)}) copy-start(f32[2,256]{1,0:T(2,128)} %param.24) | copy-start | bytes 6148
  151.1 5.9 %copy-start.7 = (f32[512,1,256]{2,0,1:T(8,128)S(1)}, f32[512,1,256]{2,0,1:T(8,128)}, u32[]{:S(2)}) copy-start(f32[512,1,256]{2,0,1:T(8,128)} %get-tuple-element.233) | copy-start | bytes 1572868
  151.1 6.1 %copy-start.6 = (f32[512,1,256]{2,0,1:T(8,128)S(1)}, f32[512,1,256]{2,0,1:T(8,128)}, u32[]{:S(2)}) copy-start(f32[512,1,256]{2,0,1:T(8,128)} %get-tuple-element.234) | copy-start | bytes 1572868
  152.9 8.4 %all-to-all-start = ((f32[4,1,512]{2,1,0:T(1,128)}), f32[4,1,512]{2,1,0:T(1,128)S(1)}, u32[]{:S(2)}, u32[]{:S(2)}) async-start(f32[4,1,512]{2,1,0:T(1,128)} %broadcast_in_dim.32), calls=%async_computation | async-start | bytes 16384 | tf_op jit(solution)/shard_map/all_to_all | solution.py:68
  157.5 6.2 %copy-start.8 = (bf16[2,256,2048]{2,1,0:T(8,128)(2,1)S(1)}, bf16[2,256,2048]{2,1,0:T(8,128)(2,1)}, u32[]{:S(2)}) copy-start(bf16[2,256,2048]{2,1,0:T(8,128)(2,1)} %param.25) | copy-start | bytes 6291460
  166.5 19.0 %all-to-all-start.2 = ((bf16[4,128,2048]{2,1,0:T(8,128)(2,1)}), bf16[4,128,2048]{2,1,0:T(8,128)(2,1)S(1)}, u32[]{:S(2)}, u32[]{:S(2)}) async-start(bf16[4,128,2048]{2,1,0:T(8,128)(2,1)} %bitcast.1002), calls=%async_computation.2 | async-start | bytes 4194304 | tf_op jit(solution)/shard_map/all_to_all | solution.py:85
  170.3 17.2 %copy-start.49 = (f32[2048]{0:T(1024)S(1)}, f32[2048]{0:T(1024)}, u32[]{:S(2)}) copy-start(f32[2048]{0:T(1024)} %param.26) | copy-start | bytes 24580
  (43 other events, 96.2 us)
Sparse Core Ops, SparseCore 0:
  42.5 59.4 all-gather.8
  103.9 113.8 all-gather.6
where the time goes:
time: 279 us; the launch traced here: 274 us
  waiting for transfers between devices  78.4 us (28%)
  blocking collectives  69 us (25%)
  local copies, waits for them, and re-layouts  45.6 us (16%)
  matrix products  33.2 us (12%)
  other arithmetic  20.6 us (7%)
  between operations  14.9 us (5%)
  starting transfers between devices  12 us (4%)
    all_gather x1, waiting for transfers between devices, collected_together(): both, at, found = (lax.all_gather(jnp.concatenate(lines), axis), 0, {})  51 us
    squeeze x54, local copies, waits for them, and re-layouts, prefix_by_axis(): so_far = combine(so_far, jax.tree.map(lambda part: part[k], pieces))  27.9 us
    all_to_all x1, blocking collectives, sum_at_owner(): blocks = lax.all_to_all(in_blocks(value, dim, size), axis, 0, 0, tiled=True)  25.9 us
    all_gather x1, blocking collectives, collected_together(): both, at, found = (lax.all_gather(jnp.concatenate(lines), axis), 0, {})  22.3 us
    all_to_all x1, blocking collectives, from_everyone(): lax.all_to_all(jnp.broadcast_to(value[None], (size, *value.shape)), axis,...  20.9 us
    all_to_all x1, waiting for transfers between devices, sum_at_owner(): blocks = lax.all_to_all(in_blocks(value, dim, size), axis, 0, 0, tiled=True)  15.3 us
    dot_general x1, matrix products, local(): ffn_term = jnp.dot(active, down_whole, preferred_element_type=jnp.float32)  13.3 us
    all_gather x1, waiting for transfers between devices, rows_first(): lax.all_gather(both, axis, axis=0, tiled=True)  9 us
  transfers between devices with their start and end apart: 5, of which 4 were waited for; matrix products, arithmetic and copies ran while one was open for 22% of the time, Pallas kernels for 0%

commit v1 on v0

v1 whole, which is shorter than its diff:
```python
import functools

import jax
import jax.numpy as jnp
from jax import lax
from jax.experimental import pallas as pl
from jax.experimental.pallas import tpu as pltpu
from jax.sharding import PartitionSpec as P

F32 = jnp.float32
BF16 = jnp.bfloat16
HIGHEST = lax.Precision.HIGHEST
EPS = 1e-06
NEG = -1e30
LANES = 128
PIECE = 16
INTERPRET = False


def iota(shape, dim):
    return lax.broadcasted_iota(jnp.int32, shape, dim)


def dot(a, b, ca=1, cb=0, precision=None):
    return lax.dot_general(
        a, b, (((ca,), (cb,)), ((), ())), preferred_element_type=F32, precision=precision
    )


def call(kernel, name, out_shape, flops, nbytes, scratch=(), **kw):
    return pl.pallas_call(
        kernel,
        name=name,
        out_shape=out_shape,
        scratch_shapes=scratch,
        interpret=INTERPRET,
        cost_estimate=pl.CostEstimate(flops=flops, bytes_accessed=nbytes, transcendentals=0),
        **kw,
    )


def sds(shape, dtype):
    return jax.ShapeDtypeStruct(shape, dtype)


def state_kernel(ka_ref, kb_ref, v_ref, in_ref, forget_ref, out_ref, cum_ref, held):
    length = ka_ref.shape[0]
    f = forget_ref[...]
    ls = jnp.minimum(f, 0.0) - jnp.log1p(jnp.exp(-jnp.abs(f)))
    upto = (iota((length, length), 0) <= iota((length, length), 1)).astype(F32)
    cum = dot(ls, upto, precision=HIGHEST)
    cum_ref[...] = cum
    total = cum[:, length - 1 : length]
    tail = total - cum + in_ref[...]
    peak = jnp.max(tail, axis=1, keepdims=True)
    weight = jnp.exp(tail - peak)
    by_row = jnp.transpose(weight)
    first = iota((LANES, LANES), 1) < LANES // 2
    first_row = iota((1, LANES), 1) < LANES // 2
    ka = ka_ref[...]

    def weighted(n):
        v = v_ref[:, n * LANES : (n + 1) * LANES].astype(F32)
        return (v * by_row[:, n : n + 1]).astype(BF16)

    held[0] = jnp.where(first, dot(weighted(0), ka, 0, 0), dot(weighted(1), ka, 0, 0))
    na = dot(weight, ka.astype(F32), precision=HIGHEST)
    norms = [jnp.where(first_row, na[0:1], na[1:2])]
    for h in range(2):
        kb = kb_ref[:, h * LANES : (h + 1) * LANES]
        held[1 + h] = dot(weighted(2 + h), kb, 0, 0)
        norms.append(dot(weight, kb.astype(F32), precision=HIGHEST)[2 + h : 3 + h])
    row, lane = iota((8, LANES), 0), iota((8, LANES), 1)
    scalars = jnp.where(lane == row, total, 0.0) + jnp.where(lane == row + 8, peak, 0.0)
    norms.append(jnp.sum(scalars, axis=0, keepdims=True))
    last = jnp.concatenate(norms, axis=0)
    for j in range(out_ref.shape[0]):
        for m in range(3):
            out_ref[j, 4 * m : 4 * m + 4, :] = held[m, 4 * j : 4 * j + 4, :]
        out_ref[j, 12:16, :] = last


def fold_kernel(r_ref, o_ref, w_ref):
    n = r_ref.shape[0]
    scalars = jnp.transpose(r_ref[:, 15, :])
    e, a = scalars[0:8], scalars[8:16]
    j = iota((8, n), 1)
    row, lane = iota((8, LANES), 0), iota((8, LANES), 1)
    gap = jnp.zeros((8, n), F32)
    for i in range(n):
        if i == 0:
            peak = jnp.full((8, 1), NEG, F32)
            w_ref[i] = jnp.zeros((8, n), F32)
        else:
            gap = jnp.where(j < i - 1, gap + e[:, i - 1 : i], 0.0)
            level = jnp.where(j < i, gap + a, -jnp.inf)
            peak = jnp.maximum(jnp.max(level, axis=1, keepdims=True), NEG)
            w_ref[i] = jnp.exp(level - peak)
        o_ref[i, 15:16, :] = jnp.sum(jnp.where(lane == row, peak, 0.0), axis=0, keepdims=True)
    first = iota((n, 5 * LANES), 1) % LANES < LANES // 2
    for m in range(3):
        rows = [4 * m, 4 * m + 1, 4 * m + 2, 4 * m + 3, 12 + m]
        x = jnp.concatenate([r_ref[:, r, :] for r in rows], axis=1)
        if m == 0:
            y = jnp.where(
                first,
                dot(w_ref[:, 0, :], x, precision=HIGHEST),
                dot(w_ref[:, 1, :], x, precision=HIGHEST),
            )
        else:
            y = dot(w_ref[:, 1 + m, :], x, precision=HIGHEST)
        for k, r in enumerate(rows):
            o_ref[:, r, :] = y[:, k * LANES : (k + 1) * LANES]


def read_kernel(
    scales,
    qa_ref,
    ka_ref,
    qb_ref,
    kb_ref,
    v_ref,
    gate_ref,
    gain_ref,
    in_ref,
    cum_ref,
    p_ref,
    y_ref,
    held,
):
    length = qa_ref.shape[0]
    rows = 128
    for j in range(p_ref.shape[0]):
        for m in range(3):
            held[m, 4 * j : 4 * j + 4, :] = p_ref[j, 4 * m : 4 * m + 4, :]
    cum_col = jnp.transpose(cum_ref[...])
    lane_half = iota((rows, LANES), 1) < LANES // 2
    states = []
    for m in range(3):
        state = held[m]
        high = state.astype(BF16)
        states.append((high, (state - high.astype(F32)).astype(BF16)))
    for at in range(0, length, rows):
        seen = at + rows
        causal = iota((rows, seen), 0) + at >= iota((rows, seen), 1)
        squares = []
        for group in range(2):
            square = None
            for h in range(2):
                n = 2 * group + h
                m = 0 if group == 0 else 1 + h
                if group == 0:
                    q = qa_ref[at : at + rows, :]
                    q = jnp.where(lane_half == (h == 0), q, jnp.zeros_like(q))
                    k = ka_ref[0:seen, :]
                else:
                    q = qb_ref[at : at + rows, h * LANES : (h + 1) * LANES]
                    k = kb_ref[0:seen, h * LANES : (h + 1) * LANES]
                scale = scales[group]
                start = p_ref[0, 15:16, n : n + 1]
                c = cum_col[at : at + rows, n : n + 1]
                level = c - cum_ref[n : n + 1, 0:seen] + in_ref[n : n + 1, 0:seen]
                level = jnp.where(causal, level, -jnp.inf)
                carried = c + start
                peak = jnp.maximum(carried, jnp.max(level, axis=1, keepdims=True))
                p = dot(q, k, 1, 1) * scale * jnp.exp(level - peak)
                before = jnp.exp(carried - peak) * scale
                reach = jnp.sum(q.astype(F32) * p_ref[0, 12 + m : 13 + m, :], axis=1, keepdims=True)
                den = jnp.sum(p, axis=1, keepdims=True) + before * reach
                v = v_ref[0:seen, n * LANES : (n + 1) * LANES]
                high, low = states[m]
                num = dot(p.astype(BF16), v) + before * (dot(q, high, 1, 1) + dot(q, low, 1, 1))
                cell = num / jnp.maximum(jnp.abs(den), jnp.exp(-peak))
                part = jnp.sum(cell * cell, axis=1, keepdims=True)
                square = part if square is None else square + part
                columns = slice(n * LANES, (n + 1) * LANES)
                gate = gate_ref[at : at + rows, columns].astype(F32)
                y = cell * gain_ref[0:1, columns] / (1.0 + jnp.exp(-gate))
                y_ref[at : at + rows, columns] = y.astype(BF16)
            squares.append(square)
        lane = iota((rows, LANES), 1)
        extra = jnp.zeros((rows, LANES), F32)
        for group in range(2):
            left = squares[group]
            for k in range(3):
                piece = left.astype(BF16).astype(F32)
                extra = jnp.where(lane == 3 * group + k, piece, extra)
                left = left - piece
        y_ref[at : at + rows, 4 * LANES :] = extra.astype(BF16)


def project_kernel(
    where_ref, y_ref, own_ref, *refs
):
    tp, rows, _ = y_ref.shape
    mine_refs, other_refs = refs[0 : tp - 1], refs[tp - 1 : 2 * tp - 2]
    stream_ref, gain_ref, res_ref, out_ref = refs[2 * tp - 2 :]
    step = pl.program_id(0)
    width = own_ref.shape[2]
    half = own_ref.shape[1]
    me, core = where_ref[0], where_ref[1]
    total = jnp.zeros((rows, LANES), F32)
    for j in range(tp):
        total = total + y_ref[j, :, 2 * half :].astype(F32)
    group_columns = tp * half
    norms = []
    for g in range(2):
        square = jnp.sum(total[:, 3 * g : 3 * g + 3], axis=1, keepdims=True)
        norms.append(lax.rsqrt(square / group_columns + EPS))
    y = y_ref[me]
    sums = [dot(y[:, g * half : (g + 1) * half], own_ref[g]) for g in range(2)]
    even = core == 0
    same = jnp.zeros((rows, width), F32)
    cross = jnp.zeros((rows, width), F32)
    for d in range(1, tp):
        y = y_ref[lax.rem(me + d, tp)]
        first, second = y[:, 0:half], y[:, half : 2 * half]
        same = same + dot(jnp.where(even, first, second), mine_refs[d - 1][...])
        cross = cross + dot(jnp.where(even, second, first), other_refs[d - 1][...])
    mix = norms[0] * (sums[0] + jnp.where(even, same, cross))
    mix = mix + norms[1] * (sums[1] + jnp.where(even, cross, same))
    columns = pl.ds(pl.multiple_of(step * width, width), width)
    res_ref[:, columns] = stream_ref[...].astype(F32) + mix

    @pl.when(step == pl.num_programs(0) - 1)
    def _():
        residual = res_ref[...]
        mean = jnp.mean(residual * residual, axis=1, keepdims=True)
        out_ref[...] = (residual * lax.rsqrt(mean + EPS) * gain_ref[...]).astype(BF16)


def hidden_kernel(tiles, x_ref, w_ref, o_ref, buf, sems):
    hidden = w_ref.shape[1] // 2
    copies = []
    for t, (at, size) in enumerate(tiles):
        for part in range(2):
            copy = pltpu.make_async_copy(
                w_ref.at[:, pl.ds(part * hidden + at, size)],
                buf.at[:, pl.ds(part * hidden + at, size)],
                sems.at[t, part],
            )
            copy.start()
            copies.append(copy)
    for t, (at, size) in enumerate(tiles):
        copies[2 * t].wait()
        copies[2 * t + 1].wait()
        gate = dot(x_ref[...], buf[:, at : at + size])
        up = dot(x_ref[...], buf[:, hidden + at : hidden + at + size])
        o_ref[:, at : at + size] = (gate / (1.0 + jnp.exp(-gate)) * up).astype(BF16)


def down_kernel(h_ref, w_ref, o_ref):
    o_ref[...] = dot(h_ref[...], w_ref[...], 1, 1).astype(BF16)


def tiles_of(total, size):
    return [(at, min(size, total - at)) for at in range(0, total, size)]


def state_and_read(qa, ka, qb, kb, v, gate, gain, in_rates, forget_rates, exchange, blocks, halves):
    length = qa.shape[0]
    pieces = sds((blocks, PIECE, LANES), F32)
    held = pltpu.VMEM((3, LANES, LANES), F32)
    own, cum = call(
        state_kernel,
        "state",
        (pieces, sds((8, length), F32)),
        4 * 2 * length * LANES * LANES,
        2 << 20,
        [held],
    )(ka, kb, v, in_rates, forget_rates)
    folded = call(
        fold_kernel,
        "fold",
        pieces,
        1 << 24,
        1 << 20,
        [pltpu.VMEM((blocks, 8, blocks), F32)],
    )(exchange(own))
    before, halves = lax.optimization_barrier((exchange(folded), halves))
    scales = ((LANES // 2) ** -0.5, LANES**-0.5)
    y = call(
        functools.partial(read_kernel, scales),
        "read",
        sds((length, 5 * LANES), BF16),
        4 * 4 * length * length * LANES,
        3 << 20,
        [held],
    )(qa, ka, qb, kb, v, gate, gain, in_rates, cum, before)
    return y, halves


def local(
    stream,
    queries_a,
    keys_a,
    queries_b,
    keys_b,
    values,
    out_gate,
    in_gate,
    forget_gate,
    head_gain,
    out_weight,
    norm_gain,
    gate_weight,
    up_weight,
    down_weight,
):
    tp, sp = lax.axis_size("tp"), lax.axis_size("sp")
    me, core = lax.axis_index("tp"), lax.axis_index("sp") % 2
    length, model = stream.shape
    hidden = gate_weight.shape[1]
    share = length // tp

    both = lax.all_gather(
        jnp.concatenate([gate_weight, up_weight], axis=1), "sp", axis=0, tiled=True
    )
    down = lax.all_gather(jnp.transpose(down_weight), "sp", axis=0, tiled=True)

    half = lax.dynamic_index_in_dim(out_weight, core, 0, keepdims=False)
    mine = [
        lax.ppermute(half, "tp", [((i + d) % tp, i) for i in range(tp)]) for d in range(1, tp)
    ]

    def eight(rates):
        rates = rates.reshape(4, length)
        return jnp.concatenate([rates, rates], axis=0)

    def exchange(pieces):
        return lax.all_to_all(pieces, "sp", 0, 0, tiled=True)

    y, mine = state_and_read(
        queries_a,
        keys_a,
        queries_b,
        keys_b,
        values.reshape(length, -1),
        out_gate.reshape(length, -1),
        head_gain.reshape(1, -1),
        eight(in_gate),
        eight(forget_gate),
        exchange,
        sp,
        mine,
    )
    other = [lax.ppermute(m, "sp", [(i, i ^ 1) for i in range(sp)]) for m in mine]
    y = lax.all_to_all(y.reshape(tp, share, -1), "tp", 0, 0, tiled=True)
    width = 512
    quarter = out_weight.shape[1]
    residual, normed = call(
        project_kernel,
        "project",
        (sds((share, model), F32), sds((share, model), BF16)),
        2 * share * model * model,
        10 << 20,
        grid_spec=pltpu.PrefetchScalarGridSpec(
            num_scalar_prefetch=1,
            grid=(model // width,),
            in_specs=[
                pl.BlockSpec(y.shape, lambda n, s: (0, 0, 0)),
                pl.BlockSpec((2, quarter, width), lambda n, s: (0, 0, n)),
                *([pl.BlockSpec((quarter, width), lambda n, s: (0, n))] * (2 * tp - 2)),
                pl.BlockSpec((share, width), lambda n, s: (s[0], n)),
                pl.BlockSpec((1, model), lambda n, s: (0, 0)),
            ],
            out_specs=[
                pl.BlockSpec((share, model), lambda n, s: (0, 0)),
                pl.BlockSpec((share, model), lambda n, s: (0, 0)),
            ],
        ),
    )(jnp.stack([me, core]).astype(jnp.int32), y, out_weight, *mine, *other, stream, norm_gain[None])
    rows = lax.all_to_all(
        jnp.broadcast_to(normed[None], (tp, share, model)), "tp", 0, 0, tiled=True
    ).reshape(length, model)
    tiles = tiles_of(hidden, 256)
    active = call(
        functools.partial(hidden_kernel, tiles),
        "hidden",
        sds((length, hidden), BF16),
        4 * length * model * hidden,
        16 << 20,
        [pltpu.VMEM((model, 2 * hidden), BF16), pltpu.SemaphoreType.DMA((len(tiles), 2))],
        in_specs=[
            pl.BlockSpec(memory_space=pltpu.VMEM),
            pl.BlockSpec(memory_space=pl.ANY),
        ],
    )(rows, both)
    block = 512
    term = call(
        down_kernel,
        "down",
        sds((length, model), BF16),
        2 * length * model * hidden,
        8 << 20,
        grid=(model // block,),
        in_specs=[
            pl.BlockSpec((length, hidden), lambda n: (0, 0)),
            pl.BlockSpec((block, hidden), lambda n: (n, 0)),
        ],
        out_specs=pl.BlockSpec((length, block), lambda n: (0, n)),
    )(active, down)
    parts = lax.all_to_all(term.reshape(tp, share, model), "tp", 0, 0, tiled=True)
    return (residual + jnp.sum(parts.astype(F32), axis=0)).astype(BF16)


def solution(mesh):
    rows, cols = ("grp", "sp"), "tp"
    return jax.shard_map(
        local,
        mesh=mesh,
        in_specs=(
            P(rows, None),
            P(rows, cols),
            P(rows, cols),
            P(rows, cols),
            P(rows, cols),
            P(rows, None, cols),
            P(rows, None, cols),
            P(None, cols, rows),
            P(None, cols, rows),
            P(None, cols),
            P(None, cols, None),
            P(),
            P("sp", cols),
            P("sp", cols),
            P(cols, "sp"),
        ),
        out_specs=P(("grp", "sp", "tp"), None),
        check_vma=False,
    )
```

time: 279 us -> 247 us (0.89); the launches traced: 274 us -> 247 us
  Pallas kernels: 0 us -> 43 us
  local copies, waits for them, and re-layouts: 45.6 us -> 8.26 us
  matrix products: 33.2 us -> 0 us
  starting transfers between devices: 12 us -> 39.2 us
  other arithmetic: 20.6 us -> 4.52 us
  blocking collectives: 69 us -> 58.4 us
    pallas_call x0 -> x6, Pallas kernels: none -> 43 us  [the longest x1 12 us: local(): call(functools.partial(hidden_kernel, tiles), 'hidden', sds((length, hidd...]
    all_gather x2, waiting for transfers between devices: 60 us -> 23 us  [the longest x1 23 us: local(): down = lax.all_gather(jnp.transpose(down_weight), 'sp', axis=0, tiled=True)]
    dot_general x16 -> x0, matrix products: 33.2 us -> none  [the longest x1 13.3 us: local(): ffn_term = jnp.dot(active, down_whole, preferred_element_type=jnp.float32)]
    squeeze x54 -> x1, local copies, waits for them, and re-layouts: 27.9 us -> 1.04 us  [local(): half = lax.dynamic_index_in_dim(out_weight, core, 0, keepdims=False)]
    all_to_all x3, starting transfers between devices: 12 us -> 34.3 us  [the longest x2 30 us: exchange(): return lax.all_to_all(pieces, 'sp', 0, 0, tiled=True)]
    all_gather x1 -> x0, blocking collectives: 22.3 us -> none  [collected_together(): both, at, found = (lax.all_gather(jnp.concatenate(lines), axis), 0, {})]
    ppermute x0 -> x6, waiting for transfers between devices: none -> 20.4 us  [the longest x3 20.4 us: local(): lax.ppermute(half, 'tp', [((i + d) % tp, i) for i in range(tp)])]
    all_to_all x3, waiting for transfers between devices: 18.2 us -> 35.4 us  [the longest x2 25.4 us: exchange(): return lax.all_to_all(pieces, 'sp', 0, 0, tiled=True)]
  transfers between devices with their start and end apart: 5 -> 11, of which waited for: 4 -> 6; matrix products, arithmetic and copies ran while one was open for 22% -> 3% of each run, Pallas kernels for 0% -> 14%
where the time goes in v1:
time: 247 us
  waiting for transfers between devices  79.6 us (32%)
  blocking collectives  58.4 us (24%)
  Pallas kernels  43 us (17%)
  starting transfers between devices  39.2 us (16%)
  between operations  13.5 us (5%)
  local copies, waits for them, and re-layouts  8.26 us (3%)
  other arithmetic  4.52 us (2%)
    all_to_all x2, starting transfers between devices, exchange(): return lax.all_to_all(pieces, 'sp', 0, 0, tiled=True)  30 us
    all_to_all x1, blocking collectives, local(): lax.all_to_all(term.reshape(tp, share, model), 'tp', 0, 0, tiled=True)  29.8 us
    all_to_all x1, blocking collectives, local(): lax.all_to_all(jnp.broadcast_to(normed[None], (tp, share, model)), 'tp',...  28.5 us
    all_to_all x2, waiting for transfers between devices, exchange(): return lax.all_to_all(pieces, 'sp', 0, 0, tiled=True)  25.4 us
    all_gather x1, waiting for transfers between devices, local(): down = lax.all_gather(jnp.transpose(down_weight), 'sp', axis=0, tiled=True)  23 us
    ppermute x3, waiting for transfers between devices, local(): lax.ppermute(half, 'tp', [((i + d) % tp, i) for i in range(tp)])  20.4 us
    pallas_call x1, Pallas kernels, local(): call(functools.partial(hidden_kernel, tiles), 'hidden', sds((length, hidd...  12 us
    pallas_call x1, Pallas kernels, state_and_read(): call(functools.partial(read_kernel, scales), 'read', sds((length, 5 * LAN...  10 us
  transfers between devices with their start and end apart: 11, of which 6 were waited for; matrix products, arithmetic and copies ran while one was open for 3% of the time, Pallas kernels for 14%

profile of v1, /device:TPU:33, one launch (start us, length us, event | category | flops | bytes accessed | tf_op | source)
XLA Modules:
  0.0 246.5 jit_solution(2326975392244420155)
XLA Ops:
  6.6 2.0 pad_maximum_fusion
  8.7 0.7 all-gather.5.cloned.1.call-update
  9.4 1.9 copy.16
  11.4 0.6 pad_maximum_fusion.1
  12.0 3.8 %state.1 = (f32[32,16,128]{2,1,0:T(8,128)}, f32[8,512]{1,0:T(8,128)}) custom-call(bf16[512,128]{1,0:T(8,128)(2,1)} %ka_ref.3, bf16[512,256]{1,0:T(8,128)(2,1)} %kb_ref.3, bf16[512,512]{1,0:T(8,128)(2,1)} %bitcast.16, f32[8,512]{1,0:T(8,128)} %get-tuple-element.21.in_ref, f32[8,512]{1,0:T(8,128)} %get-tuple-element.22.forget_ref), custom_call_target="tpu_custom_call" | custom-call | flops 67108864 | bytes 2097152 | tf_op jit(solution)/shard_map/state/pallas_call | solution.py:264
  15.8 25.5 %all-to-all-start = ((f32[32,16,128]{2,1,0:T(8,128)}), f32[32,16,128]{2,1,0:T(8,128)S(1)}, u32[]{:S(2)}, u32[]{:S(2)}) async-start(f32[32,16,128]{2,1,0:T(8,128)} %get-tuple-element.14), calls=%async_computation | async-start | bytes 524288 | tf_op jit(solution)/shard_map/all_to_all | solution.py:331
  41.3 1.0 dynamic-slice_bitcast_fusion
  42.3 2.9 %collective-permute-start = (bf16[256,2048]{1,0:T(8,128)(2,1)}, bf16[256,2048]{1,0:T(8,128)(2,1)S(1)}, u32[]{:S(2)}, u32[]{:S(2)}) collective-permute-start(bf16[256,2048]{1,0:T(8,128)(2,1)} %dynamic-slice_bitcast_fusion), channel_id=1, source_target_pairs={{1,0},{2,1},{3,2},{0,3},{5,4},{6,5},{7,6},{4,7},{9,8},{10,9},{11,1... | collective-permute-start | bytes 3145736 | tf_op jit(solution)/shard_map/ppermute | solution.py:323
  45.4 0.7 collective-permute-start.2
  46.2 20.2 %all-to-all-done.r_ref = f32[32,16,128]{2,1,0:T(8,128)S(1)} async-done(((f32[32,16,128]{2,1,0:T(8,128)}), f32[32,16,128]{2,1,0:T(8,128)S(1)}, u32[]{:S(2)}, u32[]{:S(2)}) %all-to-all-start) | async-done | bytes 262176 | tf_op jit(solution)/shard_map/all_to_all | solution.py:331
  66.4 0.7 copy-done.6
  67.1 2.5 fold.1
  69.6 4.5 %all-to-all-start.1 = ((f32[32,16,128]{2,1,0:T(8,128)}), f32[32,16,128]{2,1,0:T(8,128)S(1)}, u32[]{:S(2)}, u32[]{:S(2)}) async-start(f32[32,16,128]{2,1,0:T(8,128)} %fold.1), calls=%async_computation.1 | async-start | bytes 524288 | tf_op jit(solution)/shard_map/all_to_all | solution.py:331
  74.1 15.6 %collective-permute-done.refs_0_ = bf16[256,2048]{1,0:T(8,128)(2,1)S(1)} collective-permute-done((bf16[256,2048]{1,0:T(8,128)(2,1)}, bf16[256,2048]{1,0:T(8,128)(2,1)S(1)}, u32[]{:S(2)}, u32[]{:S(2)}) %collective-permute-start) | collective-permute-done | bytes 1048608 | tf_op jit(solution)/shard_map/ppermute | solution.py:323
  89.7 4.8 %collective-permute-done.2.refs_2_ = bf16[256,2048]{1,0:T(8,128)(2,1)} collective-permute-done((bf16[256,2048]{1,0:T(8,128)(2,1)}, bf16[256,2048]{1,0:T(8,128)(2,1)}, u32[]{:S(2)}, u32[]{:S(2)}) %collective-permute-start.2) | collective-permute-done | bytes 1048608 | tf_op jit(solution)/shard_map/ppermute | solution.py:323
  94.5 5.2 %all-to-all-done.1.p_ref = f32[32,16,128]{2,1,0:T(8,128)S(1)} async-done(((f32[32,16,128]{2,1,0:T(8,128)}), f32[32,16,128]{2,1,0:T(8,128)S(1)}, u32[]{:S(2)}, u32[]{:S(2)}) %all-to-all-start.1) | async-done | bytes 262176 | tf_op jit(solution)/shard_map/all_to_all | solution.py:331
  100.6 0.9 copy.17
  101.6 0.6 copy.18
  102.2 10.0 %read.1 = bf16[512,640]{1,0:T(8,128)(2,1)} custom-call(bf16[512,128]{1,0:T(8,128)(2,1)} %qa_ref.1, bf16[512,128]{1,0:T(8,128)(2,1)} %ka_ref.3, bf16[512,256]{1,0:T(8,128)(2,1)} %qb_ref.1, bf16[512,256]{1,0:T(8,128)(2,1)} %kb_ref.3, bf16[512,512]{1,0:T(8,128)(2,1)} %bitcast.17, bf16[512,512]{1,0:T(8,128)(2,1)} %bitcast.21, f32[1,512]{1,0:T(1,128)} %bitcast.26, ...), custom_call_target="tpu_custom_call" | custom-call | flops 536870912 | bytes 3145728 | tf_op jit(solution)/shard_map/read/pallas_call | solution.py:282
  112.2 4.3 %all-to-all-start.2 = ((bf16[4,128,640]{2,1,0:T(8,128)(2,1)}), bf16[4,128,640]{2,1,0:T(8,128)(2,1)S(1)}, u32[]{:S(2)}, u32[]{:S(2)}) async-start(bf16[4,128,640]{2,1,0:T(8,128)(2,1)} %bitcast.18), calls=%async_computation.2 | async-start | bytes 1310720 | tf_op jit(solution)/shard_map/all_to_all | solution.py:348
  116.6 0.7 pad_add_fusion.where_ref
  117.2 10.0 %all-to-all-done.2.y_ref = bf16[4,128,640]{2,1,0:T(8,128)(2,1)S(1)} async-done(((bf16[4,128,640]{2,1,0:T(8,128)(2,1)}), bf16[4,128,640]{2,1,0:T(8,128)(2,1)S(1)}, u32[]{:S(2)}, u32[]{:S(2)}) %all-to-all-start.2) | async-done | bytes 655392 | tf_op jit(solution)/shard_map/all_to_all | solution.py:348
  127.2 0.9 copy-done.1
  128.1 7.4 %project.1 = (f32[128,2048]{1,0:T(8,128)}, bf16[128,2048]{1,0:T(8,128)(2,1)}) custom-call(s32[2]{0:T(128)} %pad_add_fusion.where_ref, bf16[4,128,640]{2,1,0:T(8,128)(2,1)} %copy-done.1, bf16[2,256,2048]{2,1,0:T(8,128)(2,1)} %own_ref.1, bf16[256,2048]{1,0:T(8,128)(2,1)} %copy-done.2, bf16[256,2048]{1,0:T(8,128)(2,1)} %copy-done.3, ...), custom_call_target="tpu_custom_call" | custom-call | flops 1073741824 | bytes 10485760 | tf_op jit(solution)/shard_map/project/pallas_call | solution.py:351
  135.5 1.3 broadcast_in_dim.10
  136.8 28.5 %all_to_all.25 = bf16[4,128,2048]{2,1,0:T(8,128)(2,1)} all-to-all(bf16[4,128,2048]{2,1,0:T(8,128)(2,1)S(1)} %broadcast_in_dim.10), channel_id=1, replica_groups=mesh['grp'=2,'sp'=32,'tp'=4] {'tp'}, dimensions={0} | all-to-all | bytes 4194304 | tf_op jit(solution)/shard_map/all_to_all | solution.py:373
  165.3 12.0 %hidden.1.h_ref = bf16[512,1408]{1,0:T(8,128)(2,1)} custom-call(bf16[512,2048]{1,0:T(8,128)(2,1)} %bitcast.19, bf16[2048,2816]{1,0:T(8,128)(2,1)} %all-gather.3.cloned.1.call-done.w_ref), custom_call_target="tpu_custom_call" | custom-call | flops 5905580032 | bytes 16777216 | tf_op jit(solution)/shard_map/hidden/pallas_call | solution.py:377
  177.4 23.0 %all-gather.5.cloned.1.call-done.w_ref = bf16[2048,1408]{1,0:T(8,128)(2,1)} async-done(((bf16[64,1408]{1,0:T(8,128)(2,1)}), bf16[2048,1408]{1,0:T(8,128)(2,1)}) %all-gather.5.cloned.1.call-update) | async-done | bytes 5767184 | tf_op jit(solution)/shard_map/all_gather | solution.py:319
  200.4 7.4 %down.1 = bf16[512,2048]{1,0:T(8,128)(2,1)} custom-call(bf16[512,1408]{1,0:T(8,128)(2,1)} %hidden.1.h_ref, bf16[2048,1408]{1,0:T(8,128)(2,1)} %all-gather.5.cloned.1.call-done.w_ref), custom_call_target="tpu_custom_call" | custom-call | flops 2952790016 | bytes 8388608 | tf_op jit(solution)/shard_map/down/pallas_call | solution.py:390
  207.7 29.8 %all_to_all.26 = bf16[4,128,2048]{2,1,0:T(8,128)(2,1)S(1)} all-to-all(bf16[4,128,2048]{2,1,0:T(8,128)(2,1)} %bitcast.20), channel_id=1, replica_groups=mesh['grp'=2,'sp'=32,'tp'=4] {'tp'}, dimensions={0} | all-to-all | bytes 4194304 | tf_op jit(solution)/shard_map/all_to_all | solution.py:403
  237.9 0.8 copy-done.5
  238.8 0.9 add_convert_fusion
  (34 shorter events, 1.8 us)
Async XLA Ops:
  6.5 4.8 %copy-start.8 = (f32[2,2,512]{2,1,0:T(2,128)S(1)}, f32[2,2,512]{2,1,0:T(2,128)}, u32[]{:S(2)}) copy-start(f32[2,2,512]{2,1,0:T(2,128)} %param.22) | copy-start | bytes 24580
  6.5 4.8 %copy-start.9 = (f32[2,2,512]{2,1,0:T(2,128)S(1)}, f32[2,2,512]{2,1,0:T(2,128)}, u32[]{:S(2)}) copy-start(f32[2,2,512]{2,1,0:T(2,128)} %param.23) | copy-start | bytes 24580
  6.6 34.7 %copy-start = (bf16[2,256,2048]{2,1,0:T(8,128)(2,1)S(1)}, bf16[2,256,2048]{2,1,0:T(8,128)(2,1)}, u32[]{:S(2)}) copy-start(bf16[2,256,2048]{2,1,0:T(8,128)(2,1)} %own_ref.1) | copy-start | bytes 6291460
  6.6 158.7 %all-gather.3.cloned.1.call-start = ((), (), s32[]{:S(2)}) async-start(), calls=%async_computation.5 | async-start | bytes 11894784 | tf_op jit(solution)/shard_map/all_gather | solution.py:316
  8.6 191.8 %all-gather.5.cloned.1.call-start = ((), (), s32[]{:S(2)}) async-start(), calls=%async_computation.6 | async-start | bytes 5947392 | tf_op jit(solution)/shard_map/all_gather | solution.py:319
  12.0 88.6 %copy-start.7 = (bf16[512,2,256]{2,1,0:T(2,128)(2,1)S(1)}, bf16[512,2,256]{2,1,0:T(2,128)(2,1)}, u32[]{:S(2)}) copy-start(bf16[512,2,256]{2,1,0:T(2,128)(2,1)} %param.21) | copy-start | bytes 1572868
  15.8 50.6 %all-to-all-start = ((f32[32,16,128]{2,1,0:T(8,128)}), f32[32,16,128]{2,1,0:T(8,128)S(1)}, u32[]{:S(2)}, u32[]{:S(2)}) async-start(f32[32,16,128]{2,1,0:T(8,128)} %get-tuple-element.14), calls=%async_computation | async-start | bytes 524288 | tf_op jit(solution)/shard_map/all_to_all | solution.py:331
  41.3 60.3 %copy-start.10 = (f32[2,256]{1,0:T(2,128)S(1)}, f32[2,256]{1,0:T(2,128)}, u32[]{:S(2)}) copy-start(f32[2,256]{1,0:T(2,128)} %param.24) | copy-start | bytes 6148
  42.3 47.3 %collective-permute-start = (bf16[256,2048]{1,0:T(8,128)(2,1)}, bf16[256,2048]{1,0:T(8,128)(2,1)S(1)}, u32[]{:S(2)}, u32[]{:S(2)}) collective-permute-start(bf16[256,2048]{1,0:T(8,128)(2,1)} %dynamic-slice_bitcast_fusion), channel_id=1, source_target_pairs={{1,0},{2,1},{3,2},{0,3},{5,4},{6,5},{7,6},{4,7},{9,8},{10,9},{11,1... | collective-permute-start | bytes 3145736 | tf_op jit(solution)/shard_map/ppermute | solution.py:323
  45.2 44.5 %collective-permute-start.1 = (bf16[256,2048]{1,0:T(8,128)(2,1)}, bf16[256,2048]{1,0:T(8,128)(2,1)S(1)}, u32[]{:S(2)}, u32[]{:S(2)}) collective-permute-start(bf16[256,2048]{1,0:T(8,128)(2,1)} %dynamic-slice_bitcast_fusion), channel_id=1, source_target_pairs={{2,0},{3,1},{0,2},{1,3},{6,4},{7,5},{4,6},{5,7},{10,8},{11,9},{8,1... | collective-permute-start | bytes 3145736 | tf_op jit(solution)/shard_map/ppermute | solution.py:323
  45.4 49.0 %collective-permute-start.2 = (bf16[256,2048]{1,0:T(8,128)(2,1)}, bf16[256,2048]{1,0:T(8,128)(2,1)}, u32[]{:S(2)}, u32[]{:S(2)}) collective-permute-start(bf16[256,2048]{1,0:T(8,128)(2,1)} %dynamic-slice_bitcast_fusion), channel_id=1, source_target_pairs={{3,0},{0,1},{1,2},{2,3},{7,4},{4,5},{5,6},{6,7},{11,8},{8,9},{9,10... | collective-permute-start | bytes 3145736 | tf_op jit(solution)/shard_map/ppermute | solution.py:323
  66.4 0.7 copy-start.6
  69.6 30.1 %all-to-all-start.1 = ((f32[32,16,128]{2,1,0:T(8,128)}), f32[32,16,128]{2,1,0:T(8,128)S(1)}, u32[]{:S(2)}, u32[]{:S(2)}) async-start(f32[32,16,128]{2,1,0:T(8,128)} %fold.1), calls=%async_computation.1 | async-start | bytes 524288 | tf_op jit(solution)/shard_map/all_to_all | solution.py:331
  89.7 22.6 %copy-start.2 = (bf16[256,2048]{1,0:T(8,128)(2,1)}, bf16[256,2048]{1,0:T(8,128)(2,1)S(1)}, u32[]{:S(2)}) copy-start(bf16[256,2048]{1,0:T(8,128)(2,1)S(1)} %collective-permute-done.refs_0_) | copy-start | bytes 3145732
  89.7 22.6 %copy-start.3 = (bf16[256,2048]{1,0:T(8,128)(2,1)}, bf16[256,2048]{1,0:T(8,128)(2,1)S(1)}, u32[]{:S(2)}) copy-start(bf16[256,2048]{1,0:T(8,128)(2,1)S(1)} %collective-permute-done.1.refs_1_) | copy-start | bytes 3145732
  99.7 2.5 %copy-start.4 = (f32[32,16,128]{2,1,0:T(8,128)}, f32[32,16,128]{2,1,0:T(8,128)S(1)}, u32[]{:S(2)}) copy-start(f32[32,16,128]{2,1,0:T(8,128)S(1)} %all-to-all-done.1.p_ref) | copy-start | bytes 786436
  99.7 27.6 %collective-permute-start.3 = (bf16[256,2048]{1,0:T(8,128)(2,1)S(1)}, bf16[256,2048]{1,0:T(8,128)(2,1)}, u32[]{:S(2)}, u32[]{:S(2)}) collective-permute-start(bf16[256,2048]{1,0:T(8,128)(2,1)S(1)} %collective-permute-done.refs_0_), channel_id=1, source_target_pairs={{0,4},{4,0},{8,12},{12,8},{16,20},{20,16},{24,28},{28,24},{32,36},... | collective-permute-start | bytes 3145736 | tf_op jit(solution)/shard_map/ppermute | solution.py:347
  100.1 27.1 %collective-permute-start.4 = (bf16[256,2048]{1,0:T(8,128)(2,1)S(1)}, bf16[256,2048]{1,0:T(8,128)(2,1)}, u32[]{:S(2)}, u32[]{:S(2)}) collective-permute-start(bf16[256,2048]{1,0:T(8,128)(2,1)S(1)} %collective-permute-done.1.refs_1_), channel_id=1, source_target_pairs={{0,4},{4,0},{8,12},{12,8},{16,20},{20,16},{24,28},{28,24},{32,36},... | collective-permute-start | bytes 3145736 | tf_op jit(solution)/shard_map/ppermute | solution.py:347
  100.2 27.0 %collective-permute-start.5 = (bf16[256,2048]{1,0:T(8,128)(2,1)}, bf16[256,2048]{1,0:T(8,128)(2,1)}, u32[]{:S(2)}, u32[]{:S(2)}) collective-permute-start(bf16[256,2048]{1,0:T(8,128)(2,1)} %collective-permute-done.2.refs_2_), channel_id=1, source_target_pairs={{0,4},{4,0},{8,12},{12,8},{16,20},{20,16},{24,28},{28,24},{32,36},... | collective-permute-start | bytes 3145736 | tf_op jit(solution)/shard_map/ppermute | solution.py:347
  112.2 15.0 %all-to-all-start.2 = ((bf16[4,128,640]{2,1,0:T(8,128)(2,1)}), bf16[4,128,640]{2,1,0:T(8,128)(2,1)S(1)}, u32[]{:S(2)}, u32[]{:S(2)}) async-start(bf16[4,128,640]{2,1,0:T(8,128)(2,1)} %bitcast.18), calls=%async_computation.2 | async-start | bytes 1310720 | tf_op jit(solution)/shard_map/all_to_all | solution.py:348
  127.2 0.9 copy-start.1
  237.6 1.2 copy-start.5
Sparse Core Ops, SparseCore 0:
  9.2 118.8 all-gather.2
  130.0 70.3 all-gather.4

commit v2 on v0

v2 whole, which is shorter than its diff:
```python
import functools

import jax
import jax.numpy as jnp
from jax import lax
from jax.experimental import pallas as pl
from jax.experimental.pallas import tpu as pltpu
from jax.sharding import PartitionSpec as P

F32 = jnp.float32
BF16 = jnp.bfloat16
HIGHEST = lax.Precision.HIGHEST
MESH = pl.DeviceIdType.MESH
EPS = 1e-06
NEG = -1e30
LANES = 128
HALF = LANES // 2
STATE_PIECES = ((0, 8 + HALF), (8 + HALF, HALF), (8 + 2 * HALF, HALF))
STATE_ROWS = 8 + 3 * HALF


def iota(shape, dim):
    return lax.broadcasted_iota(jnp.int32, shape, dim)


def dot(a, b, ca=1, cb=0, precision=None):
    return lax.dot_general(
        a, b, (((ca,), (cb,)), ((), ())), preferred_element_type=F32, precision=precision
    )


def sds(shape, dtype):
    return jax.ShapeDtypeStruct(shape, dtype)


def to_lanes(columns, at):
    row, lane = iota((8, LANES), 0), iota((8, LANES), 1)
    return jnp.sum(jnp.where(lane == row + at, columns, 0.0), axis=0, keepdims=True)


def layer_kernel(cfg, *refs):
    sp, tp, scales, names = cfg
    r = dict(zip(names, refs))
    nz, far = sp // 2, sp // 4
    me, t = lax.axis_index("sp"), lax.axis_index("tp")
    z, c = me // 2, lax.rem(me, 2)
    first_core = c == 0

    def chip(k):
        return lax.rem(z + (k + nz), nz)

    right, left = {"sp": chip(1) * 2 + c}, {"sp": chip(-1) * 2 + c}
    onward = {"sp": jnp.where(first_core, chip(1), chip(-1)) * 2 + c}
    sibling = {"sp": z * 2 + (1 - c)}

    def peer(d):
        return lax.rem(t + d, tp)

    sends = []

    def send(src, dst, send_sem, recv_sem, device):
        copy = pltpu.make_async_remote_copy(
            src_ref=src,
            dst_ref=dst,
            send_sem=send_sem,
            recv_sem=recv_sem,
            device_id=device,
            device_id_type=MESH,
        )
        copy.start()
        sends.append(copy)

    def arrived(dst, send_sem, recv_sem, device):
        pltpu.make_async_remote_copy(
            src_ref=dst,
            dst_ref=dst,
            send_sem=send_sem,
            recv_sem=recv_sem,
            device_id=device,
            device_id_type=MESH,
        ).wait_recv()

    barrier = pltpu.get_barrier_semaphore()
    greeted = [right, left, sibling] + [{"tp": peer(d)} for d in range(1, tp)]
    for device in greeted:
        pl.semaphore_signal(barrier, inc=1, device_id=device, device_id_type=MESH)
    pl.semaphore_wait(barrier, len(greeted))

    def ring(view, own, send_sems, recv_sems, shared):
        def hop(way, s, p, source):
            k = -s if way == 0 else s
            send(
                source if s == 0 else view(k, p),
                view(k, p),
                send_sems.at[way, s, p],
                recv_sems.at[way, s, p],
                right if way == 0 else left,
            )

        def last_hop(p, source):
            k = jnp.where(first_core, chip(1 - far), chip(far - 1))
            send(
                source if far == 1 else view(None, p, k),
                view(None, p, k),
                send_sems.at[0, far - 1, p],
                recv_sems.at[0, far - 1, p],
                onward,
            )

        def step(s, p, source=None):
            if 0 < s < far:
                for way in range(2):
                    k = -s if way == 0 else s
                    arrived(
                        view(k, p),
                        send_sems.at[way, s - 1, p],
                        recv_sems.at[way, s - 1, p],
                        right if way == 0 else left,
                    )
                    if s < far - 1:
                        hop(way, s, p, None)
                    shared(k, p, 2 * s - 1 + way)
                if s == far - 1:
                    last_hop(p, None)
            elif s == 0:
                if far > 1:
                    hop(0, 0, p, source)
                    hop(1, 0, p, source)
                else:
                    last_hop(p, source)
            else:
                arrived(
                    view(far, p),
                    send_sems.at[0, far - 1, p],
                    recv_sems.at[0, far - 1, p],
                    onward,
                )
                shared(far, p, nz - 1)

        return step

    shard_rows, hidden = r["gate_w"].shape
    wall = r["wall"]
    piece_rows = ((0, shard_rows), (0, shard_rows), (0, shard_rows // 2), (shard_rows // 2,) * 2)
    piece_cols = (0, hidden, 2 * hidden, 2 * hidden)

    def weight_view(k, p, at=None, core=None):
        at = chip(k) if at is None else at
        row = (at * 2 + (c if core is None else core)) * shard_rows + piece_rows[p][0]
        row = pl.multiple_of(row, shard_rows // 2)
        return wall.at[pl.ds(row, piece_rows[p][1]), pl.ds(piece_cols[p], hidden)]

    def own_weight(p):
        if p < 2:
            return r["gate_w"] if p == 0 else r["up_w"]
        return r["down_w"].at[pl.ds(piece_rows[p][0], piece_rows[p][1]), :]

    def weight_to_sibling(k, p, n, source=None):
        view = weight_view(k, p)
        send(
            view if source is None else source,
            view,
            r["wb_send"].at[n, p],
            r["wb_recv"].at[n, p],
            sibling,
        )

    weight_step = ring(
        weight_view, own_weight, r["w_send"], r["w_recv"], weight_to_sibling
    )
    for p in range(2):
        weight_step(0, p, own_weight(p))
    local = []
    for p in range(4):
        copy = pltpu.make_async_copy(own_weight(p), weight_view(0, p), r["own_sem"].at[p])
        copy.start()
        local.append(copy)

    ow = r["ow"]
    copy = pltpu.make_async_copy(r["out_w"], ow.at[t], r["own_sem"].at[4])
    copy.start()
    local.append(copy)
    for d in range(1, tp):
        send(
            r["out_w"].at[c],
            ow.at[t, c],
            r["o_send"].at[d - 1],
            r["o_recv"].at[d - 1],
            {"tp": peer(d)},
        )
    for p in range(2):
        weight_to_sibling(0, p, 0, own_weight(p))

    length = r["qa"].shape[0]
    f = r["forget"][...]
    ls = jnp.minimum(f, 0.0) - jnp.log1p(jnp.exp(-jnp.abs(f)))
    upto = (iota((length, length), 0) <= iota((length, length), 1)).astype(F32)
    cum = dot(ls, upto, precision=HIGHEST)
    in_rates = r["in_rates"][...]
    total = cum[:, length - 1 : length]
    tail = total - cum + in_rates
    peak = jnp.max(tail, axis=1, keepdims=True)
    weight = jnp.exp(tail - peak)
    by_row = jnp.transpose(weight)
    head_lane = iota((1, LANES), 1) < HALF
    ka = r["ka"][...]

    def weighted(n):
        v = r["v"][:, n * LANES : (n + 1) * LANES].astype(F32)
        return (v * by_row[:, n : n + 1]).astype(BF16)

    state = r["state"]
    norms = dot(weight, ka.astype(F32), precision=HIGHEST)
    norms = [jnp.where(head_lane, norms[0:1], norms[1:2])]
    state[0, 8 : 8 + LANES, :] = jnp.where(
        head_lane, dot(weighted(0), ka, 0, 0), dot(weighted(1), ka, 0, 0)
    )
    for h in range(2):
        kb = r["kb"][:, h * LANES : (h + 1) * LANES]
        at = 8 + (1 + h) * LANES
        state[0, at : at + LANES, :] = dot(weighted(2 + h), kb, 0, 0)
        norms.append(dot(weight, kb.astype(F32), precision=HIGHEST)[2 + h : 3 + h])
    norms.append(to_lanes(total, 0) + to_lanes(peak, 8))
    norms.append(jnp.zeros((4, LANES), F32))
    state[0, 0:8, :] = jnp.concatenate(norms, axis=0)
    send(state.at[0], state.at[1], r["b_send"].at[0], r["b_recv"].at[0], sibling)
    for p in range(2, 4):
        weight_to_sibling(0, p, 0, own_weight(p))

    rows = 128
    cum_col = jnp.transpose(cum)
    lane_half = iota((rows, LANES), 1) < HALF
    num_ref, den_ref, max_ref = r["num"], r["den"], r["max"]

    def query(n, at):
        if n < 2:
            q = r["qa"][at : at + rows, :]
            return jnp.where(lane_half == (n == 0), q, jnp.zeros_like(q))
        return r["qb"][at : at + rows, (n - 2) * LANES : (n - 1) * LANES]

    def inside(n, at):
        seen = at + rows
        if n < 2:
            k = r["ka"][0:seen, :]
        else:
            k = r["kb"][0:seen, (n - 2) * LANES : (n - 1) * LANES]
        causal = iota((rows, seen), 0) + at >= iota((rows, seen), 1)
        level = cum_col[at : at + rows, n : n + 1] - cum[n : n + 1, 0:seen]
        level = jnp.where(causal, level + in_rates[n : n + 1, 0:seen], -jnp.inf)
        top = jnp.max(level, axis=1, keepdims=True)
        p = dot(query(n, at), k, 1, 1) * scales[n // 2] * jnp.exp(level - top)
        den_ref[n, at : at + rows, :] = jnp.sum(p, axis=1, keepdims=True)
        max_ref[n, at : at + rows, :] = top
        v = r["v"][0:seen, n * LANES : (n + 1) * LANES]
        num_ref[n, at : at + rows, :] = dot(p.astype(BF16), v)

    units = [(n, at) for at in range(0, length, rows) for n in range(4)]

    def attend(count):
        for _ in range(min(count, len(units))):
            inside(*units.pop(0))

    attend(2)

    arrived(state.at[1], r["b_send"].at[0], r["b_recv"].at[0], sibling)
    scal = [jnp.transpose(state[k, 0:8, :])[0:16, 3:4] for k in range(2)]
    early_e = jnp.where(first_core, scal[0][0:8], scal[1][0:8])
    early_a = jnp.where(first_core, scal[0][8:16], scal[1][8:16])
    late_e = jnp.where(first_core, scal[1][0:8], scal[0][0:8])
    late_a = jnp.where(first_core, scal[1][8:16], scal[0][8:16])
    both_a = jnp.maximum(late_e + early_a, late_a)
    early_w = jnp.exp(late_e + early_a - both_a)
    late_w = jnp.exp(late_a - both_a)
    own_w = jnp.where(first_core, early_w, late_w)
    other_w = jnp.where(first_core, late_w, early_w)

    def spread(columns, m):
        if m == 0:
            return jnp.where(head_lane, columns[0:1], columns[1:2])
        return jnp.broadcast_to(columns[1 + m : 2 + m], (1, LANES))

    travel = r["travel"]
    head = []
    for m in range(3):
        wo, ws = spread(own_w, m), spread(other_w, m)
        head.append(wo * state[0, m : m + 1, :] + ws * state[1, m : m + 1, :])
        source = pl.ds(pl.multiple_of(8 + m * LANES + c * HALF, 8), HALF)
        target = slice(8 + m * HALF, 8 + (m + 1) * HALF)
        travel[z, target, :] = wo * state[0, source, :] + ws * state[1, source, :]
    head.append(to_lanes(early_e + late_e, 0) + to_lanes(both_a, 8))
    head.append(jnp.zeros((4, LANES), F32))
    travel[z, 0:8, :] = jnp.concatenate(head, axis=0)

    def state_view(k, p, at=None):
        at = chip(k) if at is None else at
        return travel.at[at, pl.ds(*STATE_PIECES[p]), :]

    state_step = ring(
        state_view, None, r["s_send"], r["s_recv"], lambda k, p, n: None
    )
    for p in range(3):
        state_step(0, p, state_view(0, p))
    for s in range(1, far + 1):
        attend(3)
        for p in range(3):
            state_step(s, p)
    attend(len(units))

    scalars = jnp.concatenate([travel[k, 3:4, :] for k in range(nz)], axis=0)
    if nz < 8:
        scalars = jnp.concatenate([scalars, jnp.zeros((8 - nz, LANES), F32)], axis=0)
    scalars = jnp.transpose(scalars)
    e, a = scalars[0:8], scalars[8:16]
    lane = iota(e.shape, 1)
    gap = jnp.zeros(e.shape, F32)
    for k in range(nz):
        gap = gap + jnp.where((lane < k) & (k < z), e[:, k : k + 1], 0.0)
    level = jnp.where(lane < z, gap + a, -jnp.inf)
    start = jnp.maximum(jnp.max(level, axis=1, keepdims=True), NEG)
    fold = jnp.exp(level - start)
    after = jnp.maximum(early_e + start, early_a)
    keep = jnp.where(first_core, 1.0, jnp.exp(early_e + start - after))
    add = jnp.where(first_core, 0.0, jnp.exp(early_a - after))
    own_start = jnp.where(first_core, start, after)
    carried = r["carried"]
    begun = []
    for m in range(3):
        target = slice(8 + m * HALF, 8 + (m + 1) * HALF)
        acc = jnp.zeros((HALF, LANES), F32)
        norm = jnp.zeros((1, LANES), F32)
        for k in range(nz):
            w = spread(fold[:, k : k + 1], m)
            acc = acc + w * travel[k, target, :]
            norm = norm + w * travel[k, m : m + 1, :]
        carried[c, m] = acc
        begun.append(norm)
    send(carried.at[c], carried.at[c], r["b_send"].at[1], r["b_recv"].at[1], sibling)
    for p in range(2):
        weight_step(1, p)
    arrived(carried.at[1 - c], r["b_send"].at[1], r["b_recv"].at[1], sibling)
    starts = []
    for m in range(3):
        wk, wa = spread(keep, m), spread(add, m)
        at = 8 + m * LANES
        early = jnp.where(first_core, state[0, at : at + LANES, :], state[1, at : at + LANES, :])
        norm = jnp.where(first_core, state[0, m : m + 1, :], state[1, m : m + 1, :])
        whole = jnp.concatenate([carried[0, m], carried[1, m]], axis=0) * wk + wa * early
        high = whole.astype(BF16)
        low = (whole - high.astype(F32)).astype(BF16)
        starts.append((high, low, begun[m] * wk + wa * norm))

    y_own, y_all = r["y_own"], r["y_all"]
    share = length // tp
    for at in range(0, length, rows):
        squares = [jnp.zeros((rows, 1), F32)] * 2
        for n in range(4):
            m = max(n - 1, 0)
            high, low, norm = starts[m]
            q = query(n, at)
            carry = cum_col[at : at + rows, n : n + 1] + own_start[n : n + 1]
            top = max_ref[n, at : at + rows, :]
            peak = jnp.maximum(carry, top)
            scale = jnp.exp(top - peak)
            before = jnp.exp(carry - peak) * scales[n // 2]
            reach = jnp.sum(q.astype(F32) * norm, axis=1, keepdims=True)
            den = scale * den_ref[n, at : at + rows, :] + before * reach
            num = scale * num_ref[n, at : at + rows, :]
            num = num + before * (dot(q, high, 1, 1) + dot(q, low, 1, 1))
            cell = num / jnp.maximum(jnp.abs(den), jnp.exp(-peak))
            squares[n // 2] = squares[n // 2] + jnp.sum(cell * cell, axis=1, keepdims=True)
            columns = slice(n * LANES, (n + 1) * LANES)
            gate = r["out_gate"][at : at + rows, columns].astype(F32)
            y = cell * r["head_gain"][0:1, columns] / (1.0 + jnp.exp(-gate))
            y_own[at : at + rows, columns] = y.astype(BF16)
        lane = iota((rows, LANES), 1)
        extra = jnp.zeros((rows, LANES), F32)
        for group in range(2):
            rest = squares[group]
            for k in range(3):
                piece = rest.astype(BF16).astype(F32)
                extra = jnp.where(lane == 3 * group + k, piece, extra)
                rest = rest - piece
        y_own[at : at + rows, 4 * LANES :] = extra.astype(BF16)

    def rows_of(ref, j, half=None):
        size = share if half is None else share // 2
        at = j * share + (0 if half is None else half * size)
        return ref.at[pl.ds(pl.multiple_of(at, share // 2), size), :]

    for d in range(1, tp):
        send(
            rows_of(y_own, peer(d)),
            y_all.at[t],
            r["y_send"].at[d - 1],
            r["y_recv"].at[d - 1],
            {"tp": peer(d)},
        )
    y_all[t] = y_own[pl.ds(pl.multiple_of(t * share, share), share), :]
    for d in range(1, tp):
        j = peer(tp - d)
        arrived(ow.at[j, c], r["o_send"].at[d - 1], r["o_recv"].at[d - 1], {"tp": j})
        send(ow.at[j, c], ow.at[j, c], r["ob_send"].at[d - 1], r["ob_recv"].at[d - 1], sibling)
    for p in range(2):
        weight_step(2, p) if far >= 2 else None
    for d in range(1, tp):
        j = peer(tp - d)
        arrived(y_all.at[j], r["y_send"].at[d - 1], r["y_recv"].at[d - 1], {"tp": j})
        arrived(ow.at[j, 1 - c], r["ob_send"].at[d - 1], r["ob_recv"].at[d - 1], sibling)
    for copy in local:
        copy.wait()

    model = r["stream"].shape[1]
    quarter = 2 * LANES
    totals = jnp.zeros((share, LANES), F32)
    for j in range(tp):
        totals = totals + y_all[j, :, 4 * LANES :].astype(F32)
    factor = []
    for g in range(2):
        square = jnp.sum(totals[:, 3 * g : 3 * g + 3], axis=1, keepdims=True)
        factor.append(lax.rsqrt(square / (tp * quarter) + EPS))
    own_rows = pl.ds(pl.multiple_of(t * share, share), share)
    width = min(512, model)
    mean = jnp.zeros((share, 1), F32)
    res = r["res"]
    for at in range(0, model, width):
        columns = slice(at, at + width)
        mix = jnp.zeros((share, width), F32)
        for g in range(2):
            acc = jnp.zeros((share, width), F32)
            for j in range(tp):
                acc = acc + dot(y_all[j, :, g * quarter : (g + 1) * quarter], ow[j, g, :, columns])
            mix = mix + factor[g] * acc
        residual = r["stream"][own_rows, columns].astype(F32) + mix
        res[:, columns] = residual
        mean = mean + jnp.sum(residual * residual, axis=1, keepdims=True)
    factor = lax.rsqrt(mean / model + EPS)
    x = r["x"]
    for at in range(0, model, width):
        columns = slice(at, at + width)
        x[own_rows, columns] = (res[:, columns] * factor * r["norm_gain"][0:1, columns]).astype(
            BF16
        )

    to_right, to_left = {"tp": peer(1)}, {"tp": peer(tp - 1)}

    def x_send(j, half, n, device):
        view = rows_of(x, j, half)
        send(view, view, r["x_send"].at[n], r["x_recv"].at[n], device)

    def x_arrived(j, half, n, device):
        arrived(rows_of(x, j, half), r["x_send"].at[n], r["x_recv"].at[n], device)

    x_send(t, 0, 0, to_right)
    x_send(t, 1, 1, to_left)
    x_send(t, 1, 2, to_right)
    x_send(t, 0, 3, to_left)
    for p in range(2):
        weight_step(3, p) if far >= 3 else None
    x_arrived(peer(tp - 1), 0, 0, to_right)
    x_send(peer(tp - 1), 0, 4, to_right)
    x_arrived(peer(1), 1, 1, to_left)
    x_send(peer(1), 1, 5, to_left)
    later = [(s, p) for s in range(4, far + 1) for p in range(2)]
    for s, p in later[0:1]:
        weight_step(s, p)
    x_arrived(peer(tp - 1), 1, 2, to_right)
    x_arrived(peer(1), 0, 3, to_left)
    for s, p in later[1:2]:
        weight_step(s, p)
    x_arrived(peer(2), 0, 4, to_right)
    x_arrived(peer(2), 1, 5, to_left)
    for s, p in later[2:]:
        weight_step(s, p)
    for p in range(2, 4):
        weight_step(0, p, own_weight(p))

    def from_sibling(p):
        for n in range(nz):
            if n == 0:
                k = 0
            elif n == nz - 1:
                k = far
            else:
                k = -((n + 1) // 2) if n % 2 else n // 2
            arrived(
                weight_view(k, p, core=1 - c), r["wb_send"].at[n, p], r["wb_recv"].at[n, p], sibling
            )

    from_sibling(0)
    from_sibling(1)
    h = r["h"]
    tile = 256
    pending = [(s, p) for s in range(1, far + 1) for p in range(2, 4)]
    for at in range(0, hidden, tile):
        size = min(tile, hidden - at)
        gate = dot(x[...], wall[:, at : at + size])
        up = dot(x[...], wall[:, hidden + at : hidden + at + size])
        h[:, at : at + size] = (gate / (1.0 + jnp.exp(-gate)) * up).astype(BF16)
        for s, p in pending[0:1]:
            weight_step(s, p)
        pending = pending[1:]
    for s, p in pending:
        weight_step(s, p)
    from_sibling(2)
    from_sibling(3)

    term, heard = r["term"], r["heard"]
    part = share // 2

    def product(j, half):
        at = pl.multiple_of(j * share + half * part, part)
        return dot(h[pl.ds(at, part), :], wall[:, 2 * hidden : 3 * hidden], 1, 1)

    def hand(slot, n, device):
        send(term.at[slot], heard.at[n], r["t_send"].at[n], r["t_recv"].at[n], device)

    def heard_from(n, device):
        arrived(heard.at[n], r["t_send"].at[n], r["t_recv"].at[n], device)

    term[0] = product(peer(2), 0).astype(BF16)
    hand(0, 0, to_right)
    term[1] = product(peer(2), 1).astype(BF16)
    hand(1, 1, to_left)
    term[2] = product(peer(1), 1).astype(BF16)
    hand(2, 2, to_right)
    term[3] = product(peer(tp - 1), 0).astype(BF16)
    hand(3, 3, to_left)
    kept = product(peer(1), 0)
    heard_from(0, to_right)
    term[4] = (kept + heard[0].astype(F32)).astype(BF16)
    hand(4, 4, to_right)
    kept = product(peer(tp - 1), 1)
    heard_from(1, to_left)
    term[5] = (kept + heard[1].astype(F32)).astype(BF16)
    hand(5, 5, to_left)
    low = res[0:part, :] + product(t, 0)
    high = res[part:, :] + product(t, 1)
    for n in (2, 4):
        heard_from(n, to_right)
    for n in (3, 5):
        heard_from(n, to_left)
    low = low + heard[4].astype(F32) + heard[3].astype(F32)
    high = high + heard[2].astype(F32) + heard[5].astype(F32)
    r["out"][0:part, :] = low.astype(BF16)
    r["out"][part:, :] = high.astype(BF16)
    for copy in sends:
        copy.wait_send()


def local(
    stream,
    queries_a,
    keys_a,
    queries_b,
    keys_b,
    values,
    out_gate,
    in_gate,
    forget_gate,
    head_gain,
    out_weight,
    norm_gain,
    gate_weight,
    up_weight,
    down_weight,
):
    tp, sp = lax.axis_size("tp"), lax.axis_size("sp")
    length, model = stream.shape
    shard_rows, hidden = gate_weight.shape
    share, nz, far = length // tp, sp // 2, sp // 4
    quarter = out_weight.shape[1]

    def eight(rates):
        rates = rates.reshape(4, length)
        return jnp.concatenate([rates, rates], axis=0)

    inputs = {
        "stream": stream,
        "qa": queries_a,
        "ka": keys_a,
        "qb": queries_b,
        "kb": keys_b,
        "v": values.reshape(length, -1),
        "out_gate": out_gate.reshape(length, -1),
        "in_rates": eight(in_gate),
        "forget": eight(forget_gate),
        "head_gain": head_gain.reshape(1, -1),
        "out_w": out_weight,
        "norm_gain": norm_gain[None],
        "gate_w": gate_weight,
        "up_w": up_weight,
        "down_w": jnp.transpose(down_weight),
    }
    dma = pltpu.SemaphoreType.DMA
    scratch = {
        "wall": pltpu.VMEM((sp * shard_rows, 3 * hidden), BF16),
        "ow": pltpu.VMEM((tp, 2, quarter, model), BF16),
        "state": pltpu.VMEM((2, 8 + 3 * LANES, LANES), F32),
        "travel": pltpu.VMEM((nz, STATE_ROWS, LANES), F32),
        "carried": pltpu.VMEM((2, 3, HALF, LANES), F32),
        "num": pltpu.VMEM((4, length, LANES), F32),
        "den": pltpu.VMEM((4, length, 1), F32),
        "max": pltpu.VMEM((4, length, 1), F32),
        "y_own": pltpu.VMEM((length, 5 * LANES), BF16),
        "y_all": pltpu.VMEM((tp, share, 5 * LANES), BF16),
        "res": pltpu.VMEM((share, model), F32),
        "x": pltpu.VMEM((length, model), BF16),
        "h": pltpu.VMEM((length, hidden), BF16),
        "term": pltpu.VMEM((6, share // 2, model), BF16),
        "heard": pltpu.VMEM((6, share // 2, model), BF16),
        "w_send": dma((2, far, 4)),
        "w_recv": dma((2, far, 4)),
        "wb_send": dma((nz, 4)),
        "wb_recv": dma((nz, 4)),
        "own_sem": dma((5,)),
        "o_send": dma((tp - 1,)),
        "o_recv": dma((tp - 1,)),
        "ob_send": dma((tp - 1,)),
        "ob_recv": dma((tp - 1,)),
        "b_send": dma((2,)),
        "b_recv": dma((2,)),
        "s_send": dma((2, far, 3)),
        "s_recv": dma((2, far, 3)),
        "y_send": dma((tp - 1,)),
        "y_recv": dma((tp - 1,)),
        "x_send": dma((6,)),
        "x_recv": dma((6,)),
        "t_send": dma((6,)),
        "t_recv": dma((6,)),
    }
    scales = (HALF**-0.5, LANES**-0.5)
    names = (*inputs, "out", *scratch)
    return pl.pallas_call(
        functools.partial(layer_kernel, (sp, tp, scales, names)),
        name="layer",
        out_shape=sds((share, model), BF16),
        in_specs=[pl.BlockSpec(memory_space=pltpu.VMEM)] * len(inputs),
        out_specs=pl.BlockSpec(memory_space=pltpu.VMEM),
        scratch_shapes=list(scratch.values()),
        compiler_params=pltpu.CompilerParams(
            collective_id=0, has_side_effects=True, vmem_limit_bytes=66_000_000
        ),
    )(*inputs.values())


def solution(mesh):
    rows, cols = ("grp", "sp"), "tp"
    return jax.shard_map(
        local,
        mesh=mesh,
        in_specs=(
            P(rows, None),
            P(rows, cols),
            P(rows, cols),
            P(rows, cols),
            P(rows, cols),
            P(rows, None, cols),
            P(rows, None, cols),
            P(None, cols, rows),
            P(None, cols, rows),
            P(None, cols),
            P(None, cols, None),
            P(),
            P("sp", cols),
            P("sp", cols),
            P(cols, "sp"),
        ),
        out_specs=P(("grp", "sp", "tp"), None),
        check_vma=False,
    )
```

time: 279 us -> 199 us (0.71); the launches traced: 274 us -> 199 us
  Pallas kernels: 0 us -> 190 us
  waiting for transfers between devices: 78.4 us -> 0 us
  blocking collectives: 69 us -> 0 us
  local copies, waits for them, and re-layouts: 45.6 us -> 8.39 us
  matrix products: 33.2 us -> 0 us
  other arithmetic: 20.6 us -> 0.62 us
  between operations: 14.9 us -> 0.01 us
  starting transfers between devices: 12 us -> 0 us
    pallas_call x0 -> x1, Pallas kernels: none -> 190 us  [local(): pl.pallas_call(functools.partial(layer_kernel, (sp, tp, scales, names)),...]
    all_gather x2 -> x0, waiting for transfers between devices: 60 us -> none  [the longest x1 51 us: collected_together(): both, at, found = (lax.all_gather(jnp.concatenate(lines), axis), 0, {})]
    all_to_all x2 -> x0, blocking collectives: 46.7 us -> none  [the longest x1 25.9 us: sum_at_owner(): blocks = lax.all_to_all(in_blocks(value, dim, size), axis, 0, 0, tiled=True)]
    dot_general x16 -> x0, matrix products: 33.2 us -> none  [the longest x1 13.3 us: local(): ffn_term = jnp.dot(active, down_whole, preferred_element_type=jnp.float32)]
    squeeze x54 -> x0, local copies, waits for them, and re-layouts: 27.9 us -> none  [prefix_by_axis(): so_far = combine(so_far, jax.tree.map(lambda part: part[k], pieces))]
    all_gather x1 -> x0, blocking collectives: 22.3 us -> none  [collected_together(): both, at, found = (lax.all_gather(jnp.concatenate(lines), axis), 0, {})]
    all_to_all x3 -> x0, waiting for transfers between devices: 18.2 us -> none  [the longest x1 15.3 us: sum_at_owner(): blocks = lax.all_to_all(in_blocks(value, dim, size), axis, 0, 0, tiled=True)]
    all_to_all x3 -> x0, starting transfers between devices: 12 us -> none  [the longest x2 8.25 us: from_everyone(): lax.all_to_all(jnp.broadcast_to(value[None], (size, *value.shape)), axis,...]
  transfers between devices with their start and end apart: 5 -> 0, of which waited for: 4 -> 0; matrix products, arithmetic and copies ran while one was open for 22% -> 0% of each run, Pallas kernels for 0% -> 0%
where the time goes in v2:
time: 199 us
  Pallas kernels  190 us (95%)
  local copies, waits for them, and re-layouts  8.39 us (4%)
    pallas_call x1, Pallas kernels, local(): pl.pallas_call(functools.partial(layer_kernel, (sp, tp, scales, names)),...  190 us
    unnamed x4, local copies, waits for them, and re-layouts  6.97 us

profile of v2, /device:TPU:33, one launch (start us, length us, event | category | flops | bytes accessed | tf_op | source)
XLA Modules:
  0.0 198.9 jit_solution(5933738219139654601)
XLA Ops:
  0.0 1.3 copy.18
  1.3 0.7 reshape.17
  2.0 0.7 reshape.18
  2.7 0.6 pad_maximum_fusion
  3.3 1.9 copy.16
  5.2 1.9 copy.17
  7.1 189.8 %layer.1 = bf16[128,2048]{1,0:T(8,128)(2,1)} custom-call(bf16[512,2048]{1,0:T(8,128)(2,1)} %refs_0_.1, bf16[512,128]{1,0:T(8,128)(2,1)} %refs_1_.1, bf16[512,128]{1,0:T(8,128)(2,1)} %refs_2_.1, bf16[512,256]{1,0:T(8,128)(2,1)} %refs_3_.1, bf16[512,256]{1,0:T(8,128)(2,1)} %refs_4_.1, bf16[512,512]{1,0:T(8,128)(2,1)} %bitcast.9, bf16[512,512]{1,0:T(8,128)(2,1)} %bitcast.10, ...), custom_call_target="tpu_custom_call" | custom-call | tf_op jit(solution)/shard_map/layer/pallas_call | solution.py:633
  197.0 1.9 copy.20
